TPU v7x, 32 devices: a whole 2x2x4 slice. The times are simulated.
32 devices in a mesh: ep: 8 (over z, x), tp: 4 (over y, core).
Axes of the slice: x: 2, y: 2, z: 4, core: 2. Of those that a mesh axis runs over, the one named last changes fastest.
Arguments:
- query_rows: bfloat16 [3072, 1024], P('ep', 'tp'), may hold values from -8 to 8
- key_rows: bfloat16 [3072, 256], P('ep'), may hold values from -8 to 8
- value_rows: bfloat16 [3072, 256], P('ep'), may hold values from -6 to 6
- query_gain: float32 [64], replicated, may hold values from 0.3 to 6
- key_gain: float32 [64], replicated, may hold values from 0.3 to 6
- out_weight: bfloat16 [1024, 2048], P('tp'), may hold values from -0.1875 to 0.1875
- mixer_gain: float32 [2048], replicated, may hold values from 0.1 to 1.9
- expert_input: bfloat16 [2048, 2048], P('ep'), may hold values from -6 to 6
- expert_ids: int32 [2048, 2], P('ep'), may hold values from 0 to 7, all different within a row; in each aligned block of 256 rows (0 to 255, 256 to 511, ...) at most 96 rows name the same one
- gate_score: float32 [2048, 2], P('ep'), may hold values from 0.05 to 1
- expert_gain: float32 [2048], replicated, may hold values from 0.1 to 1.9
- gate_weight: bfloat16 [8, 2048, 4096], P('ep', None, 'tp'), may hold values from -0.125 to 0.125
- up_weight: bfloat16 [8, 2048, 4096], P('ep', None, 'tp'), may hold values from -0.125 to 0.125
- down_weight: bfloat16 [8, 4096, 2048], P('ep', 'tp'), may hold values from -0.09375 to 0.09375
- shared_gate: bfloat16 [2048, 2048], P(None, 'tp'), may hold values from -0.125 to 0.125
- shared_up: bfloat16 [2048, 2048], P(None, 'tp'), may hold values from -0.125 to 0.125
- shared_down: bfloat16 [2048, 2048], P('tp'), may hold values from -0.125 to 0.125
Outputs:
- mixer_out: bfloat16 [3072, 2048], P('ep')
- expert_out: bfloat16 [2048, 2048], P('ep', 'tp')
Inputs may be any that keep to these rules, and one draw needn't show every extreme that they name: `expert_ids`: each row names 2 different experts. In each aligned block of 256 rows (the rows of one device) no expert is named by more than 96 rows, a bound that some block reaches.
All inputs are finite; a program needn't handle non-finite values.
Results may differ from a plain program's by a relative error of at most 0.02.
The roundings to bfloat16 on the way count: a program that leaves them out, or rounds other values in their place, can miss the bound.
Values may be sent and summed in bfloat16 or wider, within the bound.
A program may use at most 128 MiB of HBM per device.

v0:
```python
import functools

import jax
import jax.numpy as jnp
from jax import lax
from jax.experimental import pallas as pl
from jax.experimental.pallas import tpu as pltpu
from jax.sharding import PartitionSpec as P

HEADS = 16
KV_HEADS = 4
HEAD_DIM = 64
GRID_W = 64

EPSILON = 1e-06
ROUTED_SCALE = 2.5
F32 = jnp.float32
BF16 = jnp.bfloat16
MESH = pl.DeviceIdType.MESH


def rotary_angles(position):
    grid_row = (position // GRID_W).astype(F32)
    grid_col = (position % GRID_W).astype(F32)
    quarter = HEAD_DIM // 4
    inverse = 10000.0 ** (-jnp.arange(quarter, dtype=F32) / quarter)
    return jnp.concatenate([grid_row[:, None] * inverse, grid_col[:, None] * inverse], axis=1)


def normalize_rotate(heads_in, gain_vector, angles):
    widened = heads_in.astype(F32)
    scaled = widened * lax.rsqrt(jnp.mean(widened * widened, axis=-1, keepdims=True) + EPSILON)
    scaled = scaled * gain_vector
    half_dim = scaled.shape[-1] // 2
    front_half = scaled[..., :half_dim]
    back_half = scaled[..., half_dim:]
    cosine_table = jnp.cos(angles)[:, None, :]
    sine_table = jnp.sin(angles)[:, None, :]
    turned = jnp.concatenate(
        [
            front_half * cosine_table - back_half * sine_table,
            front_half * sine_table + back_half * cosine_table,
        ],
        axis=-1,
    )
    return turned.astype(BF16)


def silu(v):
    return v / (1.0 + jnp.exp(-v))


def dot(a, b):
    return jnp.dot(a, b, preferred_element_type=F32)


def fused_kernel(
    sizes,
    kv_in, out_in, q_in, normed_in, pick_in, gain_in,
    sg_hbm, su_hbm, sd_hbm, ow_hbm, wg_hbm, wu_hbm, wd_hbm,
    mixer_ref, expert_ref,
    sg, su, sd, ow, wg, wu, wd,
    kv, att, mp, mrecv, msum, my, mo, xh, hid, po, rp, tt, ret,
    sho, shs, shr, cf, cb, cr,
    w_sem, kv_s, kv_r, d_s, d_r, f_s, f_r, sh_sem, mp_sem, my_s, my_r, mo_sem,
    p_s, p_r, r_s, r_r, c_s, c_r,
):
    n, tp_n, ny, heads, cp, lc = sizes
    me = lax.axis_index("ep")
    tp = lax.axis_index("tp")
    core = tp % 2
    y = tp // 2
    mate = tp + 1 - 2 * core
    other = 1 - core
    ra = kv_in.shape[0]
    half = ra // 2

    def send(src, dst, ssem, rsem, ep=None, t=None):
        return pltpu.make_async_remote_copy(
            src_ref=src, dst_ref=dst, send_sem=ssem, recv_sem=rsem,
            device_id=(me if ep is None else ep, tp if t is None else t), device_id_type=MESH,
        )

    def rows(block, size):
        return pl.ds(pl.multiple_of(block * size, size), size)

    def each(lo, hi, fn):
        def step(i, c):
            fn(i)
            return c
        lax.fori_loop(lo, hi, step, 0)

    weights = [
        pltpu.make_async_copy(a, b, w_sem.at[i])
        for i, (a, b) in enumerate(
            ((sg_hbm, sg), (su_hbm, su), (sd_hbm, sd), (ow_hbm, ow), (wg_hbm, wg), (wu_hbm, wu), (wd_hbm, wd))
        )
    ]
    for copy in weights:
        copy.start()

    barrier = pltpu.get_barrier_semaphore()

    def greet(s):
        pl.semaphore_signal(barrier, inc=1, device_id=((me + s) % n, tp), device_id_type=MESH)

    def greet_y(s):
        pl.semaphore_signal(barrier, inc=1, device_id=(me, (tp + 2 * s) % tp_n), device_id_type=MESH)

    each(1, n, greet)
    each(1, ny, greet_y)
    pl.semaphore_signal(barrier, inc=1, device_id=(me, mate), device_id_type=MESH)
    pl.semaphore_wait(barrier, n - 1 + ny - 1 + 1)

    def kv_copy(src, to):
        return send(kv_in, kv.at[rows(src, ra)], kv_s.at[to], kv_r.at[src], ep=to)

    def d_copy(src, to):
        return send(out_in.at[rows(to, cp)], xh.at[core, rows(src, cp)], d_s.at[to], d_r.at[src], ep=to)

    each(1, n, lambda s: kv_copy(me, (me + s) % n).start())
    each(1, n, lambda s: d_copy(me, (me + s) % n).start())

    def own_forward():
        return send(out_in.at[rows(me, cp)], xh.at[core, rows(me, cp)], f_s.at[me], f_r.at[me], t=mate)

    def forward(src):
        return send(xh.at[core, rows(src, cp)], xh.at[core, rows(src, cp)], f_s.at[src], f_r.at[src], t=mate)

    own_forward().start()
    kv[rows(me, ra), :] = kv_in[...]
    xh[core, rows(me, cp), :] = out_in[rows(me, cp), :]

    for i in range(3):
        weights[i].wait()
    normed = normed_in[...]
    sh_hidden = (silu(dot(normed, sg[...])) * dot(normed, su[...])).astype(BF16)

    def cols(tile):
        return pl.ds(pl.multiple_of(tile * lc, lc), lc)

    for q in range(ny):
        sho[q] = dot(sh_hidden, sd[:, cols(2 * q + other)]).astype(BF16)
    sh_copy = send(sho, shr, sh_sem.at[0], sh_sem.at[1], t=mate)
    sh_copy.start()
    for q in range(ny):
        shs[q] = dot(sh_hidden, sd[:, cols(2 * q + core)]).astype(BF16)

    each(1, n, lambda s: kv_copy((me + n - s) % n, me).wait_recv())
    total = kv.shape[0]
    bq = max(16, min(ra, 128 * 3072 // total // 16 * 16))
    while ra % bq:
        bq -= 16
    per_head = ra // bq

    def attend(i):
        block = q_in[pl.ds(pl.multiple_of(i * bq, bq), bq), :]
        scores = lax.dot_general(block, kv[...], (((1,), (1,)), ((), ())), preferred_element_type=F32)
        peak = jnp.max(scores, axis=1, keepdims=True)
        exponent = jnp.exp(scores - peak)
        row_total = jnp.sum(exponent, axis=1, keepdims=True)
        weighted = dot(exponent.astype(BF16), kv[...])
        att[pl.ds(pl.multiple_of((i % per_head) * bq, bq), bq),
            pl.ds(pl.multiple_of((i // per_head) * 128, 128), 128)] = (weighted / row_total).astype(BF16)

    steps = heads * per_head
    pair = 2 if steps % 2 == 0 else 1

    def attend_pair(i):
        for j in range(pair):
            attend(i * pair + j)

    each(0, steps // pair, attend_pair)

    def pass_on(s):
        src = (me + n - s) % n
        d_copy(src, me).wait_recv()
        forward(src).start()

    each(1, n, pass_on)

    weights[3].wait()
    width = mp.shape[1]
    tile = min(512, width)

    def project(t):
        at = pl.ds(pl.multiple_of(t * tile, tile), tile)
        mp[:, at] = dot(att[...], ow[:, at]).astype(BF16)

    each(0, width // tile, project)
    mp_copy = send(mp.at[rows(other, half)], mrecv, mp_sem.at[0], mp_sem.at[1], t=mate)
    mp_copy.start()

    weights[4].wait()
    weights[5].wait()
    each(0, n, lambda s: send(
        xh.at[other, rows(s, cp)], xh.at[other, rows(s, cp)], f_s.at[s], f_r.at[s], t=mate).wait_recv())
    depth = xh.shape[2]
    ft = min(256, hid.shape[1])

    def gate_up(t):
        at = pl.ds(pl.multiple_of(t * ft, ft), ft)
        gate = dot(xh[0], wg[0:depth, at]) + dot(xh[1], wg[depth:, at])
        up = dot(xh[0], wu[0:depth, at]) + dot(xh[1], wu[depth:, at])
        hid[:, at] = (silu(gate) * up).astype(BF16)

    each(0, 1, gate_up)
    mp_copy.wait_recv()
    msum[...] = (mp[rows(core, half), :].astype(F32) + mrecv[...].astype(F32)).astype(BF16)

    def my_copy(src, to):
        return send(msum, my.at[src], my_s.at[to], my_r.at[src], t=2 * to + core)

    each(1, ny, lambda s: my_copy(y, (y + s) % ny).start())
    my[y] = msum[...]
    each(1, hid.shape[1] // ft, gate_up)

    weights[6].wait()

    def p_copy(q):
        return send(po.at[q], rp.at[q], p_s.at[q], p_r.at[q], t=mate)

    def down_other(q):
        po[q] = dot(hid[...], wd[:, cols(2 * q + other)]).astype(BF16)
        p_copy(q).start()

    each(0, ny, down_other)

    def r_copy(q, src, to):
        return send(tt.at[q, rows(to, cp)], ret.at[q, rows(src, cp)], r_s.at[q, to], r_r.at[q, src], ep=to)

    def down_own(q):
        own = dot(hid[...], wd[:, cols(2 * q + core)]).astype(BF16).astype(F32)
        p_copy(q).wait_recv()
        tt[q] = (own + rp[q].astype(F32)).astype(BF16)
        each(1, n, lambda s: r_copy(q, me, (me + s) % n).start())
        ret[q, rows(me, cp), :] = tt[q, rows(me, cp), :]

    def down_step(s):
        down_own((y + s) % ny)

    each(1, ny + 1, down_step)

    each(1, ny, lambda s: my_copy((y + s) % ny, y).wait_recv())
    mixed = my[0].astype(F32)
    for j in range(1, ny):
        mixed = mixed + my[j].astype(F32)
    scale = lax.rsqrt(jnp.mean(mixed * mixed, axis=1, keepdims=True) + EPSILON)
    msum_out = (mixed * scale * gain_in[...]).astype(BF16)
    mixer_ref[rows(core, half), :] = msum_out
    mp_copy.wait_send()
    mp[rows(core, half), :] = msum_out
    mo_copy = send(mp.at[rows(core, half)], mo, mo_sem.at[0], mo_sem.at[1], t=mate)
    mo_copy.start()
    mo_copy.wait_recv()
    mixer_ref[rows(other, half), :] = mo[...]

    sh_copy.wait_recv()

    def combine(q):
        each(1, n, lambda s: r_copy(q, (me + n - s) % n, me).wait_recv())
        routed = dot(pick_in[0], ret[q]) + dot(pick_in[1], ret[q])
        return routed + shs[q].astype(F32) + shr[q].astype(F32)

    def c_copy(src, to):
        return send(cb.at[to], cr.at[src], c_s.at[to], c_r.at[src], t=2 * to + core)

    def combine_far(s):
        q = (y + s) % ny
        cb[q] = combine(q).astype(BF16)
        c_copy(y, q).start()

    each(1, ny, combine_far)
    cf[...] = combine(y)

    def collect(s):
        src = (y + s) % ny
        c_copy(src, y).wait_recv()
        cf[...] += cr[src].astype(F32)

    each(1, ny, collect)
    expert_ref[...] = cf[...].astype(BF16)

    def drain(s):
        to = (me + s) % n
        kv_copy(me, to).wait_send()
        d_copy(me, to).wait_send()
        forward((me + s) % n).wait_send()
        each(0, ny, lambda q: r_copy(q, me, to).wait_send())

    each(1, n, drain)
    own_forward().wait_send()
    sh_copy.wait_send()
    mo_copy.wait_send()
    each(0, ny, lambda q: p_copy(q).wait_send())

    def drain_y(s):
        to = (y + s) % ny
        my_copy(y, to).wait_send()
        c_copy(y, to).wait_send()

    each(1, ny, drain_y)


def body(
    query_rows, key_rows, value_rows, query_gain, key_gain, out_weight, mixer_gain,
    expert_input, expert_ids, gate_score, expert_gain,
    gate_weight, up_weight, down_weight, shared_gate, shared_up, shared_down,
):
    n = lax.axis_size("ep")
    tp_n = lax.axis_size("tp")
    ny = tp_n // 2
    me = lax.axis_index("ep")
    tp = lax.axis_index("tp")
    ra = query_rows.shape[0]
    heads = query_rows.shape[1] // HEAD_DIM
    first_kv = tp * heads // (HEADS // KV_HEADS)
    angles = rotary_angles(me * ra + jnp.arange(ra, dtype=jnp.int32))
    query_rot = normalize_rotate(query_rows.reshape(ra, heads, HEAD_DIM), query_gain, angles)
    query_rot = query_rot * BF16(HEAD_DIM ** (-0.5))
    q_in = jnp.pad(query_rot.transpose(1, 0, 2), ((0, 0), (0, 0), (0, HEAD_DIM))).reshape(heads * ra, 2 * HEAD_DIM)
    key_cols = lax.dynamic_slice_in_dim(key_rows, first_kv * HEAD_DIM, HEAD_DIM, 1)
    value_cols = lax.dynamic_slice_in_dim(value_rows, first_kv * HEAD_DIM, HEAD_DIM, 1)
    key_rot = normalize_rotate(key_cols.reshape(ra, 1, HEAD_DIM), key_gain, angles)
    kv_in = jnp.concatenate([key_rot.reshape(ra, HEAD_DIM), value_cols], axis=1)
    width = out_weight.shape[1]
    ow_pad = jnp.pad(out_weight.reshape(heads, HEAD_DIM, width), ((0, 0), (HEAD_DIM, 0), (0, 0)))
    ow_pad = ow_pad.reshape(heads * 2 * HEAD_DIM, width)
    rb, top = expert_ids.shape
    experts = n * gate_weight.shape[0]
    cap = 3 * rb * top // (2 * experts)
    cp = -(-cap // 16) * 16
    model = expert_input.shape[1]
    lc = model // tp_n
    widened = expert_input.astype(F32)
    normed = (
        widened * lax.rsqrt(jnp.mean(widened * widened, axis=1, keepdims=True) + EPSILON) * expert_gain
    ).astype(BF16)
    route_weight = gate_score / jnp.sum(gate_score, axis=1, keepdims=True) * ROUTED_SCALE
    named = expert_ids[:, :, None] == jnp.arange(experts, dtype=jnp.int32)
    member = jnp.any(named, axis=1)
    row_weight = jnp.sum(jnp.where(named, route_weight[:, :, None], 0.0), axis=1)
    before = jnp.tril(jnp.ones((rb, rb), BF16), -1)
    rank = dot(before, member.astype(BF16)).astype(jnp.int32)
    slot = jnp.where(member, rank, -1)
    chosen = slot[:, :, None] == jnp.arange(cp, dtype=jnp.int32)
    weight = jnp.where(chosen, row_weight[:, :, None], 0.0).reshape(rb, experts * cp)
    high = weight.astype(BF16)
    low = (weight - high.astype(F32)).astype(BF16)
    pick = jnp.stack([high, low])
    choose = chosen.astype(BF16).reshape(rb, experts * cp)
    own_cols = lax.dynamic_slice_in_dim(normed, (tp % 2) * (model // 2), model // 2, 1)
    outgoing = lax.dot_general(
        choose, own_cols, (((0,), (0,)), ((), ())), preferred_element_type=F32
    ).astype(BF16)

    slots = n * cp
    hidden = gate_weight.shape[2]
    sh = shared_gate.shape[1]
    vm = pltpu.VMEM
    dma = pltpu.SemaphoreType.DMA
    half = ra // 2
    vspec = pl.BlockSpec(memory_space=pltpu.VMEM)
    hspec = pl.BlockSpec(memory_space=pl.ANY)
    sizes = (n, tp_n, ny, heads, cp, lc)
    return pl.pallas_call(
        functools.partial(fused_kernel, sizes),
        out_shape=(
            jax.ShapeDtypeStruct((ra, width), BF16),
            jax.ShapeDtypeStruct((rb, lc), BF16),
        ),
        in_specs=[vspec] * 6 + [hspec] * 7,
        out_specs=(vspec, vspec),
        scratch_shapes=[
            vm((model, sh), BF16), vm((model, sh), BF16), vm((sh, model), BF16),
            vm((heads * 2 * HEAD_DIM, width), BF16),
            vm((model, hidden), BF16), vm((model, hidden), BF16), vm((hidden, model), BF16),
            vm((n * ra, 2 * HEAD_DIM), BF16),
            vm((ra, heads * 2 * HEAD_DIM), BF16),
            vm((ra, width), BF16), vm((half, width), BF16), vm((half, width), BF16),
            vm((ny, half, width), BF16), vm((half, width), BF16),
            vm((2, slots, model // 2), BF16), vm((slots, hidden), BF16),
            vm((ny, slots, lc), BF16), vm((ny, slots, lc), BF16),
            vm((ny, slots, lc), BF16), vm((ny, slots, lc), BF16),
            vm((ny, rb, lc), BF16), vm((ny, rb, lc), BF16), vm((ny, rb, lc), BF16),
            vm((rb, lc), F32), vm((ny, rb, lc), BF16), vm((ny, rb, lc), BF16),
            dma((7,)), dma((n,)), dma((n,)), dma((n,)), dma((n,)), dma((n,)), dma((n,)),
            dma((2,)), dma((2,)), dma((ny,)), dma((ny,)), dma((2,)),
            dma((ny,)), dma((ny,)), dma((ny, n)), dma((ny, n)), dma((ny,)), dma((ny,)),
        ],
        compiler_params=pltpu.CompilerParams(
            collective_id=0, has_side_effects=True, vmem_limit_bytes=64 * 1024 * 1000
        ),
        name="fused_layer",
    )(
        kv_in, outgoing, q_in, normed, pick, mixer_gain.reshape(1, width),
        shared_gate, shared_up, shared_down, ow_pad,
        gate_weight[0], up_weight[0], down_weight[0],
    )


def solution(mesh):
    in_specs = (
        P("ep", "tp"), P("ep", None), P("ep", None), P(), P(), P("tp", None), P(),
        P("ep", None), P("ep", None), P("ep", None), P(),
        P("ep", None, "tp"), P("ep", None, "tp"), P("ep", "tp", None),
        P(None, "tp"), P(None, "tp"), P("tp", None),
    )
    out_specs = (P("ep", None), P("ep", "tp"))
    return jax.shard_map(body, mesh=mesh, in_specs=in_specs, out_specs=out_specs, check_vma=False)
```

profile of v0, /device:TPU:27, one launch (start us, length us, event | category | flops | bytes accessed | tf_op | source)
XLA Modules:
  0.0 126.9 jit_solution(4137588741116508048)
XLA Ops:
  0.6 0.0 copy-start
  0.6 0.0 copy-start.6
  0.7 0.0 copy-start.8
  0.7 0.0 copy-start.9
  0.7 0.0 copy-start.5
  0.7 1.6 %fusion = f32[256]{0:T(256)S(1)} fusion(bf16[256,2048]{1,0:T(8,128)(2,1)} %param.24), kind=kLoop, calls=%fused_computation.2 | loop fusion | flops 1572608 | bytes 1049600 | tf_op jit(solution)/shard_map/reduce_sum | solution.py:337
  2.3 0.7 reduce_sum.48
  3.1 0.7 divide_multiply_fusion
  3.7 1.1 fusion.9
  4.9 0.7 fusion.21
  5.6 0.1 eq.65
  5.7 0.2 fusion.3
  5.9 0.7 select_reduce_fusion
  6.6 0.1 broadcast_multiply_fusion.1
  6.7 0.2 fusion.20
  6.9 0.0 copy-done
  6.9 0.1 constant_dynamic-slice_fusion
  7.0 0.2 pad_maximum_fusion.2
  7.2 0.1 copy.46
  7.3 0.1 fusion.11
  7.5 0.0 copy-done.5
  7.5 0.2 copy.48
  7.6 0.1 fusion.5
  7.7 0.1 fusion.6
  7.8 0.1 subtract_convert_fusion.1
  7.9 0.2 copy.52
  8.2 0.9 pad.8.clone
  9.0 0.1 copy.45
  9.2 0.7 fusion.15
  9.9 0.8 pad_maximum_fusion.1.kv_in
  10.6 0.2 bitcast_compare_fusion
  10.8 0.1 eq.62
  10.9 0.3 copy.50
  11.2 0.1 broadcast_in_dim.37
  11.2 0.3 copy.51
  11.5 0.1 subtract_convert_fusion
  11.6 0.0 copy-start.2
  11.6 0.0 copy-start.7
  11.6 0.1 fusion.7
  11.7 1.0 pad_maximum_fusion.pick_in
  12.7 0.4 copy-done.2
  13.1 0.3 fusion.2.normed_in
  13.4 0.0 copy-start.1
  13.4 1.7 %convolution_convert_fusion.out_in = bf16[768,1024]{1,0:T(8,128)(2,1)} fusion(pred[256,768]{0,1:T(32,128)(4,1)S(1)} %bitcast_compare_fusion, bf16[256,2048]{1,0:T(8,128)(2,1)S(1)} %fusion.2.normed_in, s32[]{:T(128)S(6)} %select_n.72), kind=kOutput, calls=%fused_computation.5 | convolution fusion | flops 403439616 | bytes 2293764 | tf_op jit(solution)/shard_map/dot_general | solution.py:353
  15.2 1.6 %pad.9 = bf16[4,128,2048]{2,1,0:T(8,128)(2,1)} pad(bf16[4,64,2048]{2,1,0:T(8,128)(2,1)S(1)} %bitcast.36, bf16[]{:T(256)} %constant.98.clone.1), padding=0_0x64_0x0_0 | pad | bytes 3145730 | tf_op jit(solution)/shard_map/jit(_pad)/pad | solution.py:327
  16.8 106.6 %fused_layer.1 = (bf16[384,2048]{1,0:T(8,128)(2,1)}, bf16[256,512]{1,0:T(8,128)(2,1)}) custom-call(bf16[384,128]{1,0:T(8,128)(2,1)} %pad_maximum_fusion.1.kv_in, bf16[768,1024]{1,0:T(8,128)(2,1)} %convolution_convert_fusion.out_in, bf16[1536,128]{1,0:T(8,128)(2,1)} %bitcast.35, bf16[256,2048]{1,0:T(8,128)(2,1)} %copy-done.1, ...), custom_call_target="tpu_custom_call" | custom-call | tf_op jit(solution)/shard_map/fused_layer/pallas_call | solution.py:366
  123.4 2.8 %copy.57 = bf16[384,2048]{1,0:T(8,128)(2,1)} copy(bf16[384,2048]{1,0:T(8,128)(2,1)} %get-tuple-element.20) | data formatting | bytes 3145728
  126.2 0.7 copy.58
  (17 shorter events, 0.1 us)
Async XLA Ops:
  0.6 6.2 %copy-start = (bf16[384,256]{1,0:T(8,128)(2,1)S(1)}, bf16[384,256]{1,0:T(8,128)(2,1)}, u32[]{:S(2)}) copy-start(bf16[384,256]{1,0:T(8,128)(2,1)} %param.19) | copy-start | bytes 589828
  0.6 6.7 %copy-start.6 = (bf16[384,256]{1,0:T(8,128)(2,1)S(1)}, bf16[384,256]{1,0:T(8,128)(2,1)}, u32[]{:S(2)}) copy-start(bf16[384,256]{1,0:T(8,128)(2,1)} %param.18) | copy-start | bytes 589828
  0.7 6.7 %copy-start.8 = (f32[64]{0:T(128)S(1)}, f32[64]{0:T(128)}, u32[]{:S(2)}) copy-start(f32[64]{0:T(128)} %param.21) | copy-start | bytes 772
  0.7 7.1 %copy-start.9 = (f32[64]{0:T(128)S(1)}, f32[64]{0:T(128)}, u32[]{:S(2)}) copy-start(f32[64]{0:T(128)} %param.20) | copy-start | bytes 772
  0.7 6.8 %copy-start.5 = (bf16[384,256]{1,0:T(8,128)(2,1)S(1)}, bf16[384,256]{1,0:T(8,128)(2,1)}, u32[]{:S(2)}) copy-start(bf16[384,256]{1,0:T(8,128)(2,1)} %param.17) | copy-start | bytes 589828
  11.6 1.5 %copy-start.2 = (bf16[256,2048]{1,0:T(8,128)(2,1)S(1)}, bf16[256,2048]{1,0:T(8,128)(2,1)}, u32[]{:S(2)}) copy-start(bf16[256,2048]{1,0:T(8,128)(2,1)} %param.24) | copy-start | bytes 3145732
  11.6 1.5 %copy-start.7 = (f32[2048]{0:T(1024)S(1)}, f32[2048]{0:T(1024)}, u32[]{:S(2)}) copy-start(f32[2048]{0:T(1024)} %param.27) | copy-start | bytes 24580
  13.1 2.1 %copy-start.3 = (bf16[256,2048]{1,0:T(8,128)(2,1)S(1)}, bf16[256,2048]{1,0:T(8,128)(2,1)}, u32[]{:S(2)}) copy-start(bf16[256,2048]{1,0:T(8,128)(2,1)} %param.22) | copy-start | bytes 3145732
  13.4 3.3 %copy-start.1 = (bf16[256,2048]{1,0:T(8,128)(2,1)}, bf16[256,2048]{1,0:T(8,128)(2,1)S(1)}, u32[]{:S(2)}) copy-start(bf16[256,2048]{1,0:T(8,128)(2,1)S(1)} %fusion.2.normed_in) | copy-start | bytes 3145732
  123.4 2.8 %copy-start.4 = (bf16[256,512]{1,0:T(8,128)(2,1)S(1)}, bf16[256,512]{1,0:T(8,128)(2,1)}, u32[]{:S(2)}) copy-start(bf16[256,512]{1,0:T(8,128)(2,1)} %get-tuple-element.21) | copy-start | bytes 786436
where the time goes:
time: 127 us
  Pallas kernels  107 us (84%)
  other arithmetic  9.5 us (7%)
  local copies, waits for them, and re-layouts  7.84 us (6%)
  matrix products  1.96 us (2%)
    pallas_call x1, Pallas kernels, body(): pl.pallas_call(functools.partial(fused_kernel, sizes), out_shape=(jax.Sha...  107 us
    unnamed x24, local copies, waits for them, and re-layouts  4.34 us

commit v1 on v0

--- a/solution.py
+++ b/solution.py
@@ -60,18 +60,21 @@
     sg_hbm, su_hbm, sd_hbm, ow_hbm, wg_hbm, wu_hbm, wd_hbm,
     mixer_ref, expert_ref,
     sg, su, sd, ow, wg, wu, wd,
-    kv, att, mp, mrecv, msum, my, mo, xh, hid, po, rp, tt, ret,
-    sho, shs, shr, cf, cb, cr,
-    w_sem, kv_s, kv_r, d_s, d_r, f_s, f_r, sh_sem, mp_sem, my_s, my_r, mo_sem,
-    p_s, p_r, r_s, r_r, c_s, c_r,
+    kv, att, mp, mrecv, msum, my, mo, xh, hid, po, rp, tt, yr, fin, ret,
+    sho, shs, shr, shp, shv,
+    w_sem, kv_s, kv_r, kf_s, d_s, d_r, m_s, m_r, g_s, g_r, sh_sem, v_s, v_r, mp_sem, my_s, my_r, mo_sem,
+    p_s, p_r, u_s, u_r, r_s, r_r,
 ):
-    n, tp_n, ny, heads, cp, lc = sizes
+    n, tp_n, ny, heads, cp, lc, xs = sizes
+    zs = n // xs
     me = lax.axis_index("ep")
     tp = lax.axis_index("tp")
     core = tp % 2
     y = tp // 2
     mate = tp + 1 - 2 * core
     other = 1 - core
+    my_z = me // xs
+    my_x = me % xs
     ra = kv_in.shape[0]
     half = ra // 2
 
@@ -115,30 +118,67 @@
     def kv_copy(src, to):
         return send(kv_in, kv.at[rows(src, ra)], kv_s.at[to], kv_r.at[src], ep=to)
 
+    def kv_forward(src_z, s):
+        src = src_z * xs + my_x
+        x_to = (my_x + s) % xs
+        return send(
+            kv.at[rows(src, ra)], kv.at[rows(src, ra)], kf_s.at[src_z * xs + x_to], kv_r.at[src], ep=my_z * xs + x_to)
+
+    def z_peer(s):
+        return ((my_z + s) % zs) * xs + my_x
+
+    def x_peer(s):
+        return my_z * xs + (my_x + s) % xs
+
+    each(1, zs, lambda s: kv_copy(me, z_peer(s)).start())
+    each(1, xs, lambda s: kv_copy(me, x_peer(s)).start())
+
     def d_copy(src, to):
-        return send(out_in.at[rows(to, cp)], xh.at[core, rows(src, cp)], d_s.at[to], d_r.at[src], ep=to)
-
-    each(1, n, lambda s: kv_copy(me, (me + s) % n).start())
+        return send(out_in.at[rows(to, cp)], xh.at[tp, rows(src, cp)], d_s.at[to], d_r.at[src], ep=to)
+
+    def m_copy(q, src):
+        block = xh.at[2 * q + core, rows(src, cp)]
+        return send(block, block, m_s.at[q, src], m_r.at[q, src], t=mate)
+
+    def m_arrive(q, src):
+        block = xh.at[2 * q + other, rows(src, cp)]
+        return send(block, block, m_s.at[q, src], m_r.at[q, src], t=mate)
+
+    def g_copy(by, q, src):
+        block = xh.at[2 * by + core, rows(src, cp)]
+        return send(block, block, g_s.at[q, src], g_r.at[by, src], t=2 * q + core)
+
     each(1, n, lambda s: d_copy(me, (me + s) % n).start())
 
-    def own_forward():
-        return send(out_in.at[rows(me, cp)], xh.at[core, rows(me, cp)], f_s.at[me], f_r.at[me], t=mate)
-
-    def forward(src):
-        return send(xh.at[core, rows(src, cp)], xh.at[core, rows(src, cp)], f_s.at[src], f_r.at[src], t=mate)
-
-    own_forward().start()
+    own_block = out_in.at[rows(me, cp)]
+    own_place = xh.at[tp, rows(me, cp)]
+    own_mate = send(own_block, own_place, m_s.at[y, me], m_r.at[y, me], t=mate)
+
+    def own_y(s):
+        q = (y + s) % ny
+        return send(own_block, own_place, g_s.at[q, me], g_r.at[y, me], t=2 * q + core)
+
+    own_mate.start()
+    each(1, ny, lambda s: own_y(s).start())
     kv[rows(me, ra), :] = kv_in[...]
-    xh[core, rows(me, cp), :] = out_in[rows(me, cp), :]
-
-    for i in range(3):
+    xh[tp, rows(me, cp), :] = out_in[rows(me, cp), :]
+
+    for i in range(2):
         weights[i].wait()
     normed = normed_in[...]
     sh_hidden = (silu(dot(normed, sg[...])) * dot(normed, su[...])).astype(BF16)
 
+    def kv_pass(s):
+        src_z = (my_z + zs - s) % zs
+        kv_copy(src_z * xs + my_x, me).wait_recv()
+        each(1, xs, lambda t: kv_forward(src_z, t).start())
+
+    each(1, zs, kv_pass)
+
     def cols(tile):
         return pl.ds(pl.multiple_of(tile * lc, lc), lc)
 
+    weights[2].wait()
     for q in range(ny):
         sho[q] = dot(sh_hidden, sd[:, cols(2 * q + other)]).astype(BF16)
     sh_copy = send(sho, shr, sh_sem.at[0], sh_sem.at[1], t=mate)
@@ -146,7 +186,35 @@
     for q in range(ny):
         shs[q] = dot(sh_hidden, sd[:, cols(2 * q + core)]).astype(BF16)
 
-    each(1, n, lambda s: kv_copy((me + n - s) % n, me).wait_recv())
+    def v_copy(by, q):
+        return send(shp.at[q], shv.at[by], v_s.at[q], v_r.at[by], t=2 * q + core)
+
+    sh_copy.wait_recv()
+    each(0, ny, lambda q: shp.__setitem__(q, (shs[q].astype(F32) + shr[q].astype(F32)).astype(BF16)))
+    each(1, ny, lambda s: v_copy(y, (y + s) % ny).start())
+
+    def kv_rest(s):
+        x_from = (my_x + xs - s) % xs
+        each(0, zs, lambda t: kv_copy(((my_z + t) % zs) * xs + x_from, me).wait_recv())
+
+    each(1, xs, kv_rest)
+
+    def pass_on(s):
+        src = (me + n - s) % n
+        d_copy(src, me).wait_recv()
+        m_copy(y, src).start()
+        each(1, ny, lambda t: g_copy(y, (y + t) % ny, src).start())
+
+    def pass_y(s):
+        src = (me + n - s) % n
+
+        def one(t):
+            q = (y + t) % ny
+            g_copy(q, y, src).wait_recv()
+            m_copy(q, src).start()
+
+        each(1, ny, one)
+
     total = kv.shape[0]
     bq = max(16, min(ra, 128 * 3072 // total // 16 * 16))
     while ra % bq:
@@ -165,19 +233,22 @@
 
     steps = heads * per_head
     pair = 2 if steps % 2 == 0 else 1
+    turns = steps // pair
 
     def attend_pair(i):
         for j in range(pair):
             attend(i * pair + j)
-
-    each(0, steps // pair, attend_pair)
-
-    def pass_on(s):
-        src = (me + n - s) % n
-        d_copy(src, me).wait_recv()
-        forward(src).start()
-
-    each(1, n, pass_on)
+        lo = 1 + i * (n - 1) // turns
+        hi = 1 + (i + 1) * (n - 1) // turns
+
+        def step(s):
+            pass_on(s)
+            pass_y(s - 1)
+
+        each(lo, hi, step)
+
+    each(0, turns, attend_pair)
+    pass_y(n - 1)
 
     weights[3].wait()
     width = mp.shape[1]
@@ -193,15 +264,16 @@
 
     weights[4].wait()
     weights[5].wait()
-    each(0, n, lambda s: send(
-        xh.at[other, rows(s, cp)], xh.at[other, rows(s, cp)], f_s.at[s], f_r.at[s], t=mate).wait_recv())
-    depth = xh.shape[2]
+    each(0, n, lambda s: each(0, ny, lambda q: m_arrive(q, s).wait_recv()))
     ft = min(256, hid.shape[1])
 
     def gate_up(t):
         at = pl.ds(pl.multiple_of(t * ft, ft), ft)
-        gate = dot(xh[0], wg[0:depth, at]) + dot(xh[1], wg[depth:, at])
-        up = dot(xh[0], wu[0:depth, at]) + dot(xh[1], wu[depth:, at])
+        gate = dot(xh[0], wg[0:lc, at])
+        up = dot(xh[0], wu[0:lc, at])
+        for j in range(1, tp_n):
+            gate = gate + dot(xh[j], wg[j * lc:(j + 1) * lc, at])
+            up = up + dot(xh[j], wu[j * lc:(j + 1) * lc, at])
         hid[:, at] = (silu(gate) * up).astype(BF16)
 
     each(0, 1, gate_up)
@@ -216,30 +288,55 @@
     each(1, hid.shape[1] // ft, gate_up)
 
     weights[6].wait()
-
-    def p_copy(q):
-        return send(po.at[q], rp.at[q], p_s.at[q], p_r.at[q], t=mate)
-
-    def down_other(q):
-        po[q] = dot(hid[...], wd[:, cols(2 * q + other)]).astype(BF16)
-        p_copy(q).start()
-
-    each(0, ny, down_other)
-
-    def r_copy(q, src, to):
-        return send(tt.at[q, rows(to, cp)], ret.at[q, rows(src, cp)], r_s.at[q, to], r_r.at[q, src], ep=to)
-
-    def down_own(q):
-        own = dot(hid[...], wd[:, cols(2 * q + core)]).astype(BF16).astype(F32)
-        p_copy(q).wait_recv()
-        tt[q] = (own + rp[q].astype(F32)).astype(BF16)
-        each(1, n, lambda s: r_copy(q, me, (me + s) % n).start())
-        ret[q, rows(me, cp), :] = tt[q, rows(me, cp), :]
-
-    def down_step(s):
-        down_own((y + s) % ny)
-
-    each(1, ny + 1, down_step)
+    hn = n // 2
+    hs = hn * cp
+    near = me // hn
+    far = 1 - near
+
+    def p_copy(hf, q):
+        return send(po.at[q, rows(hf, hs)], rp.at[q, rows(hf, hs)], p_s.at[hf, q], p_r.at[hf, q], t=mate)
+
+    def down_other(hf, q):
+        po[q, rows(hf, hs), :] = dot(hid[rows(hf, hs), :], wd[:, cols(2 * q + other)]).astype(BF16)
+        p_copy(hf, q).start()
+
+    def u_copy(by, q, to):
+        return send(tt.at[q, rows(to, cp)], yr.at[by, rows(to, cp)], u_s.at[q, to], u_r.at[by, to], t=2 * q + core)
+
+    def down_own(hf, q):
+        own = dot(hid[rows(hf, hs), :], wd[:, cols(2 * q + core)]).astype(BF16).astype(F32)
+        p_copy(hf, q).wait_recv()
+        tt[q, rows(hf, hs), :] = (own + rp[q, rows(hf, hs), :].astype(F32)).astype(BF16)
+
+    def down_away(hf, s):
+        q = (y + s) % ny
+        down_own(hf, q)
+        each(0, hn, lambda t: u_copy(y, q, hf * hn + (me + t) % hn).start())
+
+    def r_copy(src, to):
+        return send(fin.at[rows(to, cp)], ret.at[rows(src, cp)], r_s.at[to], r_r.at[src], ep=to)
+
+    def finish(to):
+        value = tt[y, rows(to, cp), :].astype(F32)
+        for t in range(1, ny):
+            q = (y + t) % ny
+            u_copy(q, y, to).wait_recv()
+            value = value + yr[q, rows(to, cp), :].astype(F32)
+        return value.astype(BF16)
+
+    def finish_send(to):
+        fin[rows(to, cp), :] = finish(to)
+        r_copy(me, to).start()
+
+    each(1, ny + 1, lambda s: down_other(far, (y + s) % ny))
+    each(1, ny, lambda s: down_away(far, s))
+    down_own(far, y)
+    each(1, ny + 1, lambda s: down_other(near, (y + s) % ny))
+    each(0, hn, lambda t: finish_send(far * hn + (me + t) % hn))
+    each(1, ny, lambda s: down_away(near, s))
+    down_own(near, y)
+    each(1, hn, lambda t: finish_send(near * hn + (me + t) % hn))
+    ret[rows(me, cp), :] = finish(me)
 
     each(1, ny, lambda s: my_copy((y + s) % ny, y).wait_recv())
     mixed = my[0].astype(F32)
@@ -255,49 +352,43 @@
     mo_copy.wait_recv()
     mixer_ref[rows(other, half), :] = mo[...]
 
-    sh_copy.wait_recv()
-
-    def combine(q):
-        each(1, n, lambda s: r_copy(q, (me + n - s) % n, me).wait_recv())
-        routed = dot(pick_in[0], ret[q]) + dot(pick_in[1], ret[q])
-        return routed + shs[q].astype(F32) + shr[q].astype(F32)
-
-    def c_copy(src, to):
-        return send(cb.at[to], cr.at[src], c_s.at[to], c_r.at[src], t=2 * to + core)
-
-    def combine_far(s):
-        q = (y + s) % ny
-        cb[q] = combine(q).astype(BF16)
-        c_copy(y, q).start()
-
-    each(1, ny, combine_far)
-    cf[...] = combine(y)
-
-    def collect(s):
-        src = (y + s) % ny
-        c_copy(src, y).wait_recv()
-        cf[...] += cr[src].astype(F32)
-
-    each(1, ny, collect)
-    expert_ref[...] = cf[...].astype(BF16)
+    shared = shs[y].astype(F32) + shr[y].astype(F32)
+    for t in range(1, ny):
+        q = (y + t) % ny
+        v_copy(q, y).wait_recv()
+        shared = shared + shv[q].astype(F32)
+    each(1, n, lambda s: r_copy((me + n - s) % n, me).wait_recv())
+    routed = dot(pick_in[0], ret[...]) + dot(pick_in[1], ret[...])
+    expert_ref[...] = (routed + shared).astype(BF16)
 
     def drain(s):
         to = (me + s) % n
-        kv_copy(me, to).wait_send()
         d_copy(me, to).wait_send()
-        forward((me + s) % n).wait_send()
-        each(0, ny, lambda q: r_copy(q, me, to).wait_send())
+        r_copy(me, to).wait_send()
+
+        def drain_src(t):
+            g_copy(y, (y + t) % ny, to).wait_send()
+            u_copy(y, (y + t) % ny, to).wait_send()
+
+        each(1, ny, drain_src)
+        each(0, ny, lambda q: m_copy(q, to).wait_send())
 
     each(1, n, drain)
-    own_forward().wait_send()
+    each(1, zs, lambda s: kv_copy(me, z_peer(s)).wait_send())
+    each(1, xs, lambda s: kv_copy(me, x_peer(s)).wait_send())
+    each(1, zs, lambda s: each(1, xs, lambda t: kv_forward((my_z + zs - s) % zs, t).wait_send()))
+    own_mate.wait_send()
     sh_copy.wait_send()
     mo_copy.wait_send()
-    each(0, ny, lambda q: p_copy(q).wait_send())
+    each(0, ny, lambda q: each(0, 2, lambda hf: p_copy(hf, q).wait_send()))
 
     def drain_y(s):
         to = (y + s) % ny
+        own_y(s).wait_send()
         my_copy(y, to).wait_send()
-        c_copy(y, to).wait_send()
+        v_copy(y, to).wait_send()
+        u_copy(y, to, me).wait_send()
+        m_copy(to, me).wait_send()
 
     each(1, ny, drain_y)
 
@@ -349,7 +440,7 @@
     low = (weight - high.astype(F32)).astype(BF16)
     pick = jnp.stack([high, low])
     choose = chosen.astype(BF16).reshape(rb, experts * cp)
-    own_cols = lax.dynamic_slice_in_dim(normed, (tp % 2) * (model // 2), model // 2, 1)
+    own_cols = lax.dynamic_slice_in_dim(normed, tp * lc, lc, 1)
     outgoing = lax.dot_general(
         choose, own_cols, (((0,), (0,)), ((), ())), preferred_element_type=F32
     ).astype(BF16)
@@ -362,7 +453,10 @@
     half = ra // 2
     vspec = pl.BlockSpec(memory_space=pltpu.VMEM)
     hspec = pl.BlockSpec(memory_space=pl.ANY)
-    sizes = (n, tp_n, ny, heads, cp, lc)
+    xs = 1
+    while 4 * xs * xs <= n:
+        xs *= 2
+    sizes = (n, tp_n, ny, heads, cp, lc, xs)
     return pl.pallas_call(
         functools.partial(fused_kernel, sizes),
         out_shape=(
@@ -379,14 +473,16 @@
             vm((ra, heads * 2 * HEAD_DIM), BF16),
             vm((ra, width), BF16), vm((half, width), BF16), vm((half, width), BF16),
             vm((ny, half, width), BF16), vm((half, width), BF16),
-            vm((2, slots, model // 2), BF16), vm((slots, hidden), BF16),
+            vm((tp_n, slots, lc), BF16), vm((slots, hidden), BF16),
             vm((ny, slots, lc), BF16), vm((ny, slots, lc), BF16),
             vm((ny, slots, lc), BF16), vm((ny, slots, lc), BF16),
+            vm((slots, lc), BF16), vm((slots, lc), BF16),
             vm((ny, rb, lc), BF16), vm((ny, rb, lc), BF16), vm((ny, rb, lc), BF16),
-            vm((rb, lc), F32), vm((ny, rb, lc), BF16), vm((ny, rb, lc), BF16),
-            dma((7,)), dma((n,)), dma((n,)), dma((n,)), dma((n,)), dma((n,)), dma((n,)),
-            dma((2,)), dma((2,)), dma((ny,)), dma((ny,)), dma((2,)),
-            dma((ny,)), dma((ny,)), dma((ny, n)), dma((ny, n)), dma((ny,)), dma((ny,)),
+            vm((ny, rb, lc), BF16), vm((ny, rb, lc), BF16),
+            dma((7,)), dma((n,)), dma((n,)), dma((n,)), dma((n,)), dma((n,)),
+            dma((ny, n)), dma((ny, n)), dma((ny, n)), dma((ny, n)),
+            dma((2,)), dma((ny,)), dma((ny,)), dma((2,)), dma((ny,)), dma((ny,)), dma((2,)),
+            dma((2, ny)), dma((2, ny)), dma((ny, n)), dma((ny, n)), dma((n,)), dma((n,)),
         ],
         compiler_params=pltpu.CompilerParams(
             collective_id=0, has_side_effects=True, vmem_limit_bytes=64 * 1024 * 1000

time: 127 us -> 122 us (0.961)
  the two profiles are of different devices: /device:TPU:27 before, /device:TPU:0 now
where the time goes in v1:
time: 122 us; the launch traced here: 121 us
  Pallas kernels  102 us (84%)
  other arithmetic  9.51 us (8%)
  local copies, waits for them, and re-layouts  7.76 us (6%)
  matrix products  1.51 us (1%)
    pallas_call x1, Pallas kernels, body(): pl.pallas_call(functools.partial(fused_kernel, sizes), out_shape=(jax.Sha...  102 us
    unnamed x24, local copies, waits for them, and re-layouts  4.29 us

profile of v1, /device:TPU:0, one launch (start us, length us, event | category | flops | bytes accessed | tf_op | source)
XLA Modules:
  0.0 121.4 jit_solution(9189908892014469986)
XLA Ops:
  0.6 0.0 copy-start
  0.6 0.0 copy-start.6
  0.7 1.6 %fusion = f32[256]{0:T(256)S(1)} fusion(bf16[256,2048]{1,0:T(8,128)(2,1)} %param.24), kind=kLoop, calls=%fused_computation.2 | loop fusion | flops 1572608 | bytes 1049600 | tf_op jit(solution)/shard_map/reduce_sum | solution.py:428
  2.3 0.7 reduce_sum.48
  3.1 0.7 divide_multiply_fusion
  3.7 1.1 fusion.9
  4.9 0.7 fusion.21
  5.6 0.1 eq.63
  5.7 0.2 fusion.3
  5.9 0.7 select_reduce_fusion
  6.6 0.1 broadcast_multiply_fusion.1
  6.7 0.2 fusion.20
  6.9 0.1 constant_dynamic-slice_fusion
  7.0 0.2 pad_maximum_fusion.2
  7.2 0.1 copy.46
  7.3 0.1 fusion.11
  7.5 0.2 copy.48
  7.6 0.1 fusion.4
  7.7 0.0 copy-done.9
  7.7 0.1 fusion.5
  7.8 0.1 subtract_convert_fusion.1
  7.9 0.2 copy.52
  8.2 0.8 pad.8.clone
  9.0 0.1 copy.45
  9.1 0.7 fusion.15
  9.8 0.8 pad_maximum_fusion.1.kv_in
  10.6 0.2 bitcast_compare_fusion
  10.8 0.1 eq.60
  10.9 0.3 copy.50
  11.1 0.1 broadcast_in_dim.37
  11.2 0.3 copy.51
  11.5 0.1 subtract_convert_fusion
  11.6 0.0 copy-start.2
  11.6 0.0 copy-start.7
  11.6 0.1 fusion.6
  11.7 0.0 copy-start.3
  11.7 1.0 pad_maximum_fusion.pick_in
  12.7 0.4 copy-done.2
  13.0 0.3 fusion.2.normed_in
  13.4 0.0 copy-start.1
  13.4 1.3 %convolution_convert_fusion.out_in = bf16[768,512]{1,0:T(8,128)(2,1)} fusion(pred[256,768]{0,1:T(32,128)(4,1)S(1)} %bitcast_compare_fusion, bf16[256,2048]{1,0:T(8,128)(2,1)S(1)} %fusion.2.normed_in, s32[]{:T(128)S(6)} %select_n.65), kind=kOutput, calls=%fused_computation.5 | convolution fusion | flops 201719808 | bytes 1245188 | tf_op jit(solution)/shard_map/dot_general | solution.py:444
  14.6 0.0 copy-done.3
  14.6 1.6 %pad.9 = bf16[4,128,2048]{2,1,0:T(8,128)(2,1)} pad(bf16[4,64,2048]{2,1,0:T(8,128)(2,1)S(1)} %bitcast.36, bf16[]{:T(256)} %constant.88.clone.1), padding=0_0x64_0x0_0 | pad | bytes 3145730 | tf_op jit(solution)/shard_map/jit(_pad)/pad | solution.py:418
  16.2 101.7 %fused_layer.1 = (bf16[384,2048]{1,0:T(8,128)(2,1)}, bf16[256,512]{1,0:T(8,128)(2,1)}) custom-call(bf16[384,128]{1,0:T(8,128)(2,1)} %pad_maximum_fusion.1.kv_in, bf16[768,512]{1,0:T(8,128)(2,1)} %convolution_convert_fusion.out_in, bf16[1536,128]{1,0:T(8,128)(2,1)} %bitcast.35, bf16[256,2048]{1,0:T(8,128)(2,1)} %copy-done.1, ...), custom_call_target="tpu_custom_call" | custom-call | tf_op jit(solution)/shard_map/fused_layer/pallas_call | solution.py:460
  117.9 0.0 copy-start.4
  117.9 2.8 %copy.57 = bf16[384,2048]{1,0:T(8,128)(2,1)} copy(bf16[384,2048]{1,0:T(8,128)(2,1)} %get-tuple-element.20) | data formatting | bytes 3145728
  120.7 0.0 copy-done.4
  120.7 0.7 copy.58
  (17 shorter events, 0.1 us)
Async XLA Ops:
  0.6 6.2 %copy-start = (bf16[384,256]{1,0:T(8,128)(2,1)S(1)}, bf16[384,256]{1,0:T(8,128)(2,1)}, u32[]{:S(2)}) copy-start(bf16[384,256]{1,0:T(8,128)(2,1)} %param.19) | copy-start | bytes 589828
  0.6 6.7 %copy-start.6 = (bf16[384,256]{1,0:T(8,128)(2,1)S(1)}, bf16[384,256]{1,0:T(8,128)(2,1)}, u32[]{:S(2)}) copy-start(bf16[384,256]{1,0:T(8,128)(2,1)} %param.18) | copy-start | bytes 589828
  0.7 6.7 %copy-start.8 = (f32[64]{0:T(128)S(1)}, f32[64]{0:T(128)}, u32[]{:S(2)}) copy-start(f32[64]{0:T(128)} %param.21) | copy-start | bytes 772
  0.7 7.1 %copy-start.9 = (f32[64]{0:T(128)S(1)}, f32[64]{0:T(128)}, u32[]{:S(2)}) copy-start(f32[64]{0:T(128)} %param.20) | copy-start | bytes 772
  0.7 6.8 %copy-start.5 = (bf16[384,256]{1,0:T(8,128)(2,1)S(1)}, bf16[384,256]{1,0:T(8,128)(2,1)}, u32[]{:S(2)}) copy-start(bf16[384,256]{1,0:T(8,128)(2,1)} %param.17) | copy-start | bytes 589828
  11.6 1.5 %copy-start.2 = (bf16[256,2048]{1,0:T(8,128)(2,1)S(1)}, bf16[256,2048]{1,0:T(8,128)(2,1)}, u32[]{:S(2)}) copy-start(bf16[256,2048]{1,0:T(8,128)(2,1)} %param.24) | copy-start | bytes 3145732
  11.6 1.5 %copy-start.7 = (f32[2048]{0:T(1024)S(1)}, f32[2048]{0:T(1024)}, u32[]{:S(2)}) copy-start(f32[2048]{0:T(1024)} %param.27) | copy-start | bytes 24580
  11.7 3.0 %copy-start.3 = (bf16[256,2048]{1,0:T(8,128)(2,1)S(1)}, bf16[256,2048]{1,0:T(8,128)(2,1)}, u32[]{:S(2)}) copy-start(bf16[256,2048]{1,0:T(8,128)(2,1)} %param.22) | copy-start | bytes 3145732
  13.4 2.9 %copy-start.1 = (bf16[256,2048]{1,0:T(8,128)(2,1)}, bf16[256,2048]{1,0:T(8,128)(2,1)S(1)}, u32[]{:S(2)}) copy-start(bf16[256,2048]{1,0:T(8,128)(2,1)S(1)} %fusion.2.normed_in) | copy-start | bytes 3145732
  117.9 2.8 %copy-start.4 = (bf16[256,512]{1,0:T(8,128)(2,1)S(1)}, bf16[256,512]{1,0:T(8,128)(2,1)}, u32[]{:S(2)}) copy-start(bf16[256,512]{1,0:T(8,128)(2,1)} %get-tuple-element.21) | copy-start | bytes 786436

commit v2 on v1

v2 whole, which is shorter than its diff:
```python
import functools

import jax
import jax.numpy as jnp
import numpy as np
from jax import lax
from jax.experimental import pallas as pl
from jax.experimental.pallas import tpu as pltpu
from jax.sharding import PartitionSpec as P

HEADS = 16
KV_HEADS = 4
HEAD_DIM = 64
GRID_W = 64

EPSILON = 1e-06
ROUTED_SCALE = 2.5
F32 = jnp.float32
BF16 = jnp.bfloat16
MESH = pl.DeviceIdType.MESH


def position_tables(grid_rows):
    quarter = HEAD_DIM // 4
    inverse = (10000.0 ** (-np.arange(quarter, dtype=np.float32) / np.float32(quarter))).astype(np.float32)
    lane = np.arange(2 * HEAD_DIM) % (2 * quarter)
    by_row = lane < quarter
    freq = inverse[lane % quarter]
    sign = np.where(np.arange(2 * HEAD_DIM) % HEAD_DIM < HEAD_DIM // 2, -1.0, 1.0).astype(np.float32)

    def pair(count, used):
        angle = np.arange(count, dtype=np.float32)[:, None] * freq
        return [np.where(used, np.cos(angle), 0.0), np.where(used, np.sin(angle) * sign, 0.0)]

    return np.concatenate(pair(GRID_W, ~by_row) + pair(grid_rows, by_row)).astype(np.float32)


def silu(v):
    return v / (1.0 + jnp.exp(-v))


def dot(a, b):
    return jnp.dot(a, b, preferred_element_type=F32)


def fused_kernel(
    sizes,
    q_ref, k_ref, v_ref, qg_ref, kg_ref, table_ref, gain_ref, x_ref, ids_ref, score_ref, xgain_ref,
    sg_hbm, su_hbm, sd_hbm, ow_hbm, wg_hbm, wu_hbm, wd_hbm,
    mixer_ref, expert_ref,
    sg, su, sd, ow, wg, wu, wd,
    kvo, kv, qs, cosv, sinv, attf, mix, nrm, cht, pick, outf, outn,
    xh, hid, po, rp, tt, yr, fin, ret, sho, shs, shr, shp, shv,
    w_sem, kv_s, kv_r, kf_s, d_s, d_r, m_s, m_r, g_s, g_r, sh_sem, v_s, v_r,
    o_s, o_r, ox_s, ox_r, om_s, om_r, a_s, a_r, am_s, am_r,
    p_s, p_r, u_s, u_r, r_s, r_r,
):
    n, tp_n, ny, heads, cp, lc, xs = sizes
    zs = n // xs
    hn = n // 2
    hs = hn * cp
    me = lax.axis_index("ep")
    tp = lax.axis_index("tp")
    core = tp % 2
    y = tp // 2
    mate = tp + 1 - 2 * core
    other = 1 - core
    my_z = me // xs
    my_x = me % xs
    near = me // hn
    far = 1 - near
    ra = k_ref.shape[0]
    rb, model = x_ref.shape
    slots = n * cp
    hr = ow_hbm.shape[0]
    pr = hr // xs
    pairs = -(-heads // 2)

    def send(src, dst, ssem, rsem, ep=None, t=None):
        return pltpu.make_async_remote_copy(
            src_ref=src, dst_ref=dst, send_sem=ssem, recv_sem=rsem,
            device_id=(me if ep is None else ep, tp if t is None else t), device_id_type=MESH,
        )

    def rows(block, size):
        return pl.ds(pl.multiple_of(block * size, size), size)

    def cols(tile):
        return pl.ds(pl.multiple_of(tile * lc, lc), lc)

    def each(lo, hi, fn):
        def step(i, c):
            fn(i)
            return c
        lax.fori_loop(lo, hi, step, 0)

    weights = [
        pltpu.make_async_copy(a, b, w_sem.at[i])
        for i, (a, b) in enumerate((
            (sg_hbm, sg), (su_hbm, su), (sd_hbm, sd), (ow_hbm, ow.at[rows(tp, hr)]),
            (wg_hbm, wg), (wu_hbm, wu), (wd_hbm, wd)))
    ]
    for copy in weights:
        copy.start()

    barrier = pltpu.get_barrier_semaphore()

    def greet(s):
        pl.semaphore_signal(barrier, inc=1, device_id=((me + s) % n, tp), device_id_type=MESH)

    def greet_y(s):
        pl.semaphore_signal(barrier, inc=1, device_id=(me, (tp + 2 * s) % tp_n), device_id_type=MESH)

    each(1, n, greet)
    each(1, ny, greet_y)
    pl.semaphore_signal(barrier, inc=1, device_id=(me, mate), device_id_type=MESH)

    def kv_copy(src, to):
        return send(kvo, kv.at[rows(src, ra)], kv_s.at[to], kv_r.at[src], ep=to)

    def kv_forward(src_z, s):
        src = src_z * xs + my_x
        x_to = (my_x + s) % xs
        return send(
            kv.at[rows(src, ra)], kv.at[rows(src, ra)], kf_s.at[src_z * xs + x_to], kv_r.at[src], ep=my_z * xs + x_to)

    def z_peer(s):
        return ((my_z + s) % zs) * xs + my_x

    def x_peer(s):
        return my_z * xs + (my_x + s) % xs

    def o_copy(q):
        return send(
            ow_hbm.at[rows(my_x, pr)], ow.at[pl.ds(pl.multiple_of(tp * hr + my_x * pr, pr), pr)],
            o_s.at[q], o_r.at[y], t=2 * q + core)

    def piece(by, x):
        return ow.at[pl.ds(pl.multiple_of((2 * by + core) * hr + x * pr, pr), pr)]

    def o_arrive(by):
        return send(piece(by, my_x), piece(by, my_x), o_s.at[by], o_r.at[by], t=2 * by + core)

    def ox_copy(by, x_to):
        return send(piece(by, my_x), piece(by, my_x), ox_s.at[by, x_to], ox_r.at[by, my_x], ep=my_z * xs + x_to)

    def ox_arrive(by, x_from):
        return send(
            piece(by, x_from), piece(by, x_from), ox_s.at[by, x_from], ox_r.at[by, x_from], ep=my_z * xs + x_from)

    def om_copy(by, side):
        tile = ow.at[rows(2 * by + side, hr)]
        return send(tile, tile, om_s.at[by], om_r.at[by], t=mate)

    pl.semaphore_wait(barrier, n - 1 + ny - 1 + 1)

    each(1, ny, lambda s: o_copy((y + s) % ny).start())

    x = x_ref[...].astype(F32)
    x_scale = lax.rsqrt(jnp.mean(x * x, axis=1, keepdims=True) + EPSILON)
    nrm[...] = (x * x_scale * xgain_ref[...]).astype(BF16)
    elane = lax.broadcasted_iota(jnp.int32, (rb, 128), 1)
    top = ids_ref.shape[1]
    named = [ids_ref[:, k:k + 1] == elane for k in range(top)]
    member = named[0]
    for k in range(1, top):
        member = member | named[k]
    earlier = lax.broadcasted_iota(jnp.int32, (rb, rb), 1) < lax.broadcasted_iota(jnp.int32, (rb, rb), 0)
    rank = dot(jnp.where(earlier, 1.0, 0.0).astype(BF16), jnp.where(member, 1.0, 0.0).astype(BF16))
    slot = jnp.where(member, rank, -1.0)
    slot_t = slot.T
    place = lax.broadcasted_iota(jnp.int32, (cp, rb), 0).astype(F32)
    for e in range(n):
        cht[e * cp:(e + 1) * cp, :] = jnp.where(slot_t[e:e + 1, :] == place, 1.0, 0.0).astype(BF16)

    def d_near(q, src, to):
        return send(
            outn.at[q, rows(to % hn, cp)], xh.at[2 * q + core, rows(src, cp)], d_s.at[q, to], d_r.at[q, src], ep=to)

    def d_far(src, to):
        return send(outf.at[rows(to % hn, cp)], xh.at[tp, rows(src, cp)], d_s.at[y, to], d_r.at[y, src], ep=to)

    def near_peer(s):
        return near * hn + (me + s) % hn

    def far_peer(s):
        return far * hn + (me + s) % hn

    for q in range(ny):
        outn[q] = dot(cht[rows(near, hs), :], nrm[:, cols(2 * q + core)]).astype(BF16)
        each(1, hn, lambda s: d_near(q, me, near_peer(s)).start())
    outf[...] = dot(cht[rows(far, hs), :], nrm[:, cols(tp)]).astype(BF16)
    each(0, hn, lambda s: d_far(me, far_peer(s)).start())
    for j in range(tp_n):
        xh[j, rows(me, cp), :] = dot(cht[rows(me, cp), :], nrm[:, j * lc:(j + 1) * lc]).astype(BF16)

    with jax.named_scope("shared"):
        for i in range(3):
            weights[i].wait()
        normed = nrm[...]
        sh_hidden = (silu(dot(normed, sg[...])) * dot(normed, su[...])).astype(BF16)
        for q in range(ny):
            sho[q] = dot(sh_hidden, sd[:, cols(2 * q + other)]).astype(BF16)
        sh_copy = send(sho, shr, sh_sem.at[0], sh_sem.at[1], t=mate)
        sh_copy.start()
        for q in range(ny):
            shs[q] = dot(sh_hidden, sd[:, cols(2 * q + core)]).astype(BF16)

    def v_copy(by, q):
        return send(shp.at[q], shv.at[by], v_s.at[q], v_r.at[by], t=2 * q + core)

    lane = lax.broadcasted_iota(jnp.int32, (1, 2 * HEAD_DIM), 1)
    left = lane < HEAD_DIM
    front = lane % HEAD_DIM < HEAD_DIM // 2
    grid_rows = (table_ref.shape[0] - 2 * GRID_W) // 2
    for g in range(ra // GRID_W):
        at = slice(g * GRID_W, (g + 1) * GRID_W)
        line = 2 * GRID_W + me * (ra // GRID_W) + g
        cosv[at, :] = table_ref[0:GRID_W, :] + table_ref[pl.ds(line, 1), :]
        sinv[at, :] = table_ref[GRID_W:2 * GRID_W, :] + table_ref[pl.ds(line + grid_rows, 1), :]

    def rotate(v):
        swapped = jnp.where(front, pltpu.roll(v, 3 * HEAD_DIM // 2, 1), pltpu.roll(v, HEAD_DIM // 2, 1))
        return v * cosv[...] + swapped * sinv[...]

    def inverse_rms(total):
        return lax.rsqrt(total * (1.0 / HEAD_DIM) + EPSILON)

    first_kv = tp * heads // (HEADS // KV_HEADS)
    kv_at = rows(first_kv // 2, 2 * HEAD_DIM)
    odd = (jnp.zeros((1, 2 * HEAD_DIM), jnp.int32) + first_kv % 2) == 1
    k_two = k_ref[:, kv_at].astype(F32)
    v_two = v_ref[:, kv_at].astype(F32)
    k_own = jnp.where(odd, pltpu.roll(k_two, HEAD_DIM, 1), k_two)
    v_own = jnp.where(odd, v_two, pltpu.roll(v_two, HEAD_DIM, 1))
    k_sum = jnp.sum(jnp.where(left, k_own * k_own, 0.0), axis=1, keepdims=True)
    k_turned = rotate(k_own * inverse_rms(k_sum) * kg_ref[...])
    kv_mine = jnp.where(left, k_turned, v_own).astype(BF16)
    kvo[...] = kv_mine
    kv[rows(me, ra), :] = kv_mine

    with jax.named_scope("queries"):
        for p in range(pairs):
            q_two = q_ref[:, p * 128:(p + 1) * 128].astype(F32)
            square = q_two * q_two
            low = inverse_rms(jnp.sum(jnp.where(left, square, 0.0), axis=1, keepdims=True))
            high = inverse_rms(jnp.sum(jnp.where(left, 0.0, square), axis=1, keepdims=True))
            turned = rotate(q_two * jnp.where(left, low, high) * qg_ref[...]) * HEAD_DIM ** (-0.5)
            qs[2 * p * ra:(2 * p + 1) * ra, :] = jnp.where(left, turned, 0.0).astype(BF16)
            if 2 * p + 1 < heads:
                qs[(2 * p + 1) * ra:(2 * p + 2) * ra, :] = jnp.where(
                    left, pltpu.roll(turned, HEAD_DIM, 1), 0.0).astype(BF16)

    with jax.named_scope("shared_pair"):
        sh_copy.wait_recv()
        for q in range(ny):
            shp[q] = (shs[q].astype(F32) + shr[q].astype(F32)).astype(BF16)
    weights[3].wait()
    om_copy(y, core).start()

    def kv_pass(s):
        src_z = (my_z + zs - s) % zs
        kv_copy(src_z * xs + my_x, me).wait_recv()
        each(1, xs, lambda t: kv_forward(src_z, t).start())

    with jax.named_scope("pick"):
        total_score = score_ref[:, 0:1]
        for k in range(1, top):
            total_score = total_score + score_ref[:, k:k + 1]
        row_weight = jnp.zeros((rb, 128), F32)
        for k in range(top):
            row_weight = row_weight + jnp.where(named[k], score_ref[:, k:k + 1] / total_score * ROUTED_SCALE, 0.0)
        high_w = row_weight.astype(BF16)
        low_w = (row_weight - high_w.astype(F32)).astype(BF16)
        slot_lane = lax.broadcasted_iota(jnp.int32, (1, slots), 1).astype(F32)
        slot_expert = jnp.floor((slot_lane + 0.5) * (1.0 / cp))
        spread = jnp.where(
            lax.broadcasted_iota(jnp.int32, (128, slots), 0).astype(F32) == slot_expert, 1.0, 0.0).astype(BF16)
        chosen = dot(slot.astype(BF16), spread) == slot_lane - slot_expert * cp
        pick[0] = jnp.where(chosen, dot(high_w, spread), 0.0).astype(BF16)
        pick[1] = jnp.where(chosen, dot(low_w, spread), 0.0).astype(BF16)

    def kv_rest(s):
        x_from = (my_x + xs - s) % xs
        each(0, zs, lambda t: kv_copy(((my_z + t) % zs) * xs + x_from, me).wait_recv())

    def m_copy(q, src):
        block = xh.at[2 * q + core, rows(src, cp)]
        return send(block, block, m_s.at[q, src], m_r.at[q, src], t=mate)

    def m_arrive(q, src):
        block = xh.at[2 * q + other, rows(src, cp)]
        return send(block, block, m_s.at[q, src], m_r.at[q, src], t=mate)

    def g_copy(by, q, src):
        block = xh.at[2 * by + core, rows(src, cp)]
        return send(block, block, g_s.at[q, src], g_r.at[by, src], t=2 * q + core)

    def near_src(s):
        return near * hn + (me + hn - s) % hn

    def far_src(s):
        return far * hn + (me + hn - s) % hn

    def near_pass(s):
        src = near_src(s)

        def one(q):
            d_near(q, src, me).wait_recv()
            m_copy(q, src).start()

        each(0, ny, one)

    def far_pass(s):
        src = far_src(s)
        d_far(src, me).wait_recv()
        each(1, ny, lambda t: g_copy(y, (y + t) % ny, src).start())
        m_copy(y, src).start()

    def far_pass_y(s):
        src = far_src(s)

        def one(t):
            q = (y + t) % ny
            g_copy(q, y, src).wait_recv()
            m_copy(q, src).start()

        each(1, ny, one)

    def ow_pass():
        def one(s):
            by = (y + s) % ny
            o_arrive(by).wait_recv()
            each(1, xs, lambda t: ox_copy(by, (my_x + t) % xs).start())

        each(1, ny, one)

    def ow_last():
        def one(s):
            by = (y + s) % ny
            each(1, xs, lambda t: ox_arrive(by, (my_x + t) % xs).wait_recv())
            om_copy(by, core).start()

        each(1, ny, one)

    total = kv.shape[0]
    bq = max(16, min(ra, 128 * 3072 // total // 16 * 16))
    while ra % bq:
        bq -= 16
    per_head = ra // bq

    def attend(head, i):
        block = qs[rows(head * per_head + i, bq), :]
        scores = lax.dot_general(block, kv[...], (((1,), (1,)), ((), ())), preferred_element_type=F32)
        peak = jnp.max(scores, axis=1, keepdims=True)
        exponent = jnp.exp(scores - peak)
        row_total = jnp.sum(exponent, axis=1, keepdims=True)
        return dot(exponent.astype(BF16), kv[...]) / row_total

    turns = pairs * per_head

    def attend_turn(i):
        p = i // per_head
        b = i % per_head
        first = attend(2 * p, b)
        if heads > 1:
            both = jnp.where(left, pltpu.roll(first, HEAD_DIM, 1), attend(2 * p + 1, b))
            attf[tp, rows(b, bq), rows(p, 128)] = both.astype(BF16)
        else:
            attf[tp, rows(b, bq), :] = first[:, HEAD_DIM:].astype(BF16)
        each(i * hn // turns, (i + 1) * hn // turns, lambda s: finish_send(far_peer(s)))

    def far_step(s):
        far_pass(s)
        each(jnp.maximum(s - 1, 0), s, far_pass_y)

    def a_copy(by, q):
        return send(attf.at[2 * by + core], attf.at[2 * by + core], a_s.at[q], a_r.at[by], t=2 * q + core)

    def am_copy(by, side):
        return send(attf.at[2 * by + side], attf.at[2 * by + side], am_s.at[by], am_r.at[by], t=mate)

    ft = min(256, hid.shape[1])

    def gate_up(hf, t):
        at = pl.ds(pl.multiple_of(t * ft, ft), ft)
        gate = dot(xh[0, rows(hf, hs), :], wg[0:lc, at])
        up = dot(xh[0, rows(hf, hs), :], wu[0:lc, at])
        for j in range(1, tp_n):
            gate = gate + dot(xh[j, rows(hf, hs), :], wg[j * lc:(j + 1) * lc, at])
            up = up + dot(xh[j, rows(hf, hs), :], wu[j * lc:(j + 1) * lc, at])
        hid[rows(hf, hs), at] = (silu(gate) * up).astype(BF16)

    def p_copy(hf, q):
        return send(po.at[q, rows(hf, hs)], rp.at[q, rows(hf, hs)], p_s.at[hf, q], p_r.at[hf, q], t=mate)

    def down_other(hf, q):
        po[q, rows(hf, hs), :] = dot(hid[rows(hf, hs), :], wd[:, cols(2 * q + other)]).astype(BF16)
        p_copy(hf, q).start()

    def u_copy(by, q, to):
        return send(tt.at[q, rows(to, cp)], yr.at[by, rows(to, cp)], u_s.at[q, to], u_r.at[by, to], t=2 * q + core)

    def down_own(hf, q):
        own = dot(hid[rows(hf, hs), :], wd[:, cols(2 * q + core)]).astype(BF16).astype(F32)
        p_copy(hf, q).wait_recv()
        tt[q, rows(hf, hs), :] = (own + rp[q, rows(hf, hs), :].astype(F32)).astype(BF16)

    def down_away(hf, s):
        q = (y + s) % ny
        down_own(hf, q)
        each(0, hn, lambda t: u_copy(y, q, hf * hn + (me + t) % hn).start())

    def r_copy(src, to):
        return send(fin.at[rows(to, cp)], ret.at[rows(src, cp)], r_s.at[to], r_r.at[src], ep=to)

    def finish(to):
        value = tt[y, rows(to, cp), :].astype(F32)
        for t in range(1, ny):
            q = (y + t) % ny
            u_copy(q, y, to).wait_recv()
            value = value + yr[q, rows(to, cp), :].astype(F32)
        return value.astype(BF16)

    def finish_send(to):
        fin[rows(to, cp), :] = finish(to)
        r_copy(me, to).start()

    def near_wait(s):
        each(0, ny, lambda q: m_arrive(q, near_src(s)).wait_recv())

    def far_wait(s):
        each(0, ny, lambda q: m_arrive(q, far_src(s)).wait_recv())

    tiles = hid.shape[1] // ft

    def near_tile(t):
        gate_up(near, t)
        each(t * hn // tiles, (t + 1) * hn // tiles, far_step)

    def far_tile(t):
        gate_up(far, t)
        each(1 + t * (zs - 1) // tiles, 1 + (t + 1) * (zs - 1) // tiles, kv_pass)

    with jax.named_scope("near_pass"):
        each(1, hn, near_pass)
    with jax.named_scope("near_wait"):
        weights[4].wait()
        weights[5].wait()
        each(1, hn, near_wait)
    each(1, zs, lambda s: kv_copy(me, z_peer(s)).start())
    each(1, xs, lambda s: kv_copy(me, x_peer(s)).start())
    with jax.named_scope("near_gate_up"):
        each(0, tiles, near_tile)
    with jax.named_scope("near_down"):
        weights[6].wait()
        each(1, ny + 1, lambda s: down_other(near, (y + s) % ny))
        far_pass_y(hn - 1)
        each(1, ny, lambda s: down_away(near, s))
        down_own(near, y)
    with jax.named_scope("far_wait"):
        each(0, hn, far_wait)
    with jax.named_scope("far_gate_up"):
        each(0, tiles, far_tile)
    with jax.named_scope("ow_pass"):
        ow_pass()
    with jax.named_scope("far_down"):
        each(1, ny + 1, lambda s: down_other(far, (y + s) % ny))
        each(1, ny, lambda s: down_away(far, s))
        down_own(far, y)
    each(1, ny, lambda s: v_copy(y, (y + s) % ny).start())
    with jax.named_scope("finish_near"):
        each(1, hn, lambda s: finish_send(near_peer(s)))
        ret[rows(me, cp), :] = finish(me)
    with jax.named_scope("kv_rest"):
        each(1, xs, kv_rest)
    with jax.named_scope("attend"):
        each(0, turns, attend_turn)
    am_copy(y, core).start()
    each(1, ny, lambda s: a_copy(y, (y + s) % ny).start())

    with jax.named_scope("ow_last"):
        ow_last()
    with jax.named_scope("att_wait"):
        def att_pass(s):
            by = (y + s) % ny
            a_copy(by, y).wait_recv()
            am_copy(by, core).start()

        each(1, ny, att_pass)
    with jax.named_scope("mixer"):
        each(0, ny, lambda by: am_copy(by, other).wait_recv())
        each(0, ny, lambda by: om_copy(by, other).wait_recv())
        width = mix.shape[1]
        tile = min(512, width)

        def project(t, ssq):
            at = pl.ds(pl.multiple_of(t * tile, tile), tile)
            part = dot(attf[0], ow[0:hr, at])
            for j in range(1, tp_n):
                part = part + dot(attf[j], ow[j * hr:(j + 1) * hr, at])
            mix[:, at] = part
            return ssq + jnp.sum(part * part, axis=1, keepdims=True)

        ssq = lax.fori_loop(0, width // tile, project, jnp.zeros((ra, 1), F32))
        scale = lax.rsqrt(ssq * (1.0 / width) + EPSILON)
        mixer_ref[...] = (mix[...] * scale * gain_ref[...]).astype(BF16)

    shared = shs[y].astype(F32) + shr[y].astype(F32)
    for t in range(1, ny):
        q = (y + t) % ny
        v_copy(q, y).wait_recv()
        shared = shared + shv[q].astype(F32)
    with jax.named_scope("ret_wait"):
        each(1, n, lambda s: r_copy((me + n - s) % n, me).wait_recv())
    expert_ref[...] = (dot(pick[0], ret[...]) + dot(pick[1], ret[...]) + shared).astype(BF16)

    def drain(s):
        to = (me + s) % n
        r_copy(me, to).wait_send()
        each(0, ny, lambda q: m_copy(q, to).wait_send())
        each(1, ny, lambda t: u_copy(y, (y + t) % ny, to).wait_send())

    def drain_far(s):
        d_far(me, far_peer(s)).wait_send()
        each(1, ny, lambda t: g_copy(y, (y + t) % ny, far_peer(s)).wait_send())

    def drain_y(s):
        q = (y + s) % ny
        o_copy(q).wait_send()
        each(1, xs, lambda t: ox_copy(q, (my_x + t) % xs).wait_send())
        a_copy(y, q).wait_send()
        v_copy(y, q).wait_send()
        u_copy(y, q, me).wait_send()

    with jax.named_scope("drain"):
        each(1, n, drain)
        each(0, hn, drain_far)
        each(1, hn, lambda s: each(0, ny, lambda q: d_near(q, me, near_peer(s)).wait_send()))
        each(1, zs, lambda s: kv_copy(me, z_peer(s)).wait_send())
        each(1, xs, lambda s: kv_copy(me, x_peer(s)).wait_send())
        each(1, zs, lambda s: each(1, xs, lambda t: kv_forward((my_z + zs - s) % zs, t).wait_send()))
        sh_copy.wait_send()
        each(0, ny, lambda q: each(0, 2, lambda hf: p_copy(hf, q).wait_send()))
        each(0, ny, lambda by: om_copy(by, core).wait_send())
        each(0, ny, lambda by: am_copy(by, core).wait_send())
        each(1, ny, drain_y)


def body(
    query_rows, key_rows, value_rows, query_gain, key_gain, out_weight, mixer_gain,
    expert_input, expert_ids, gate_score, expert_gain,
    gate_weight, up_weight, down_weight, shared_gate, shared_up, shared_down,
):
    n = lax.axis_size("ep")
    tp_n = lax.axis_size("tp")
    ny = tp_n // 2
    ra = query_rows.shape[0]
    heads = query_rows.shape[1] // HEAD_DIM
    width = out_weight.shape[1]
    rb, top = expert_ids.shape
    experts = n * gate_weight.shape[0]
    cap = 3 * rb * top // (2 * experts)
    cp = -(-cap // 16) * 16
    model = expert_input.shape[1]
    lc = model // tp_n
    xs = 1
    while 4 * xs * xs <= n:
        xs *= 2
    if heads % 2:
        query_rows = jnp.pad(query_rows, ((0, 0), (0, HEAD_DIM)))
    pairs = -(-heads // 2)
    table = jnp.asarray(position_tables(n * ra // GRID_W))
    q_gain = jnp.concatenate([query_gain, query_gain]).reshape(1, 2 * HEAD_DIM)
    k_gain = jnp.concatenate([key_gain, key_gain]).reshape(1, 2 * HEAD_DIM)

    slots = n * cp
    hidden = gate_weight.shape[2]
    sh = shared_gate.shape[1]
    hr = heads * HEAD_DIM
    vm = pltpu.VMEM
    dma = pltpu.SemaphoreType.DMA
    vspec = pl.BlockSpec(memory_space=pltpu.VMEM)
    hspec = pl.BlockSpec(memory_space=pl.ANY)
    sizes = (n, tp_n, ny, heads, cp, lc, xs)
    return pl.pallas_call(
        functools.partial(fused_kernel, sizes),
        out_shape=(
            jax.ShapeDtypeStruct((ra, width), BF16),
            jax.ShapeDtypeStruct((rb, lc), BF16),
        ),
        in_specs=[vspec] * 11 + [hspec] * 7,
        out_specs=(vspec, vspec),
        scratch_shapes=[
            vm((model, sh), BF16), vm((model, sh), BF16), vm((sh, model), BF16),
            vm((tp_n * hr, width), BF16),
            vm((model, hidden), BF16), vm((model, hidden), BF16), vm((hidden, model), BF16),
            vm((ra, 2 * HEAD_DIM), BF16), vm((n * ra, 2 * HEAD_DIM), BF16), vm((2 * pairs * ra, 2 * HEAD_DIM), BF16),
            vm((ra, 2 * HEAD_DIM), F32), vm((ra, 2 * HEAD_DIM), F32),
            vm((tp_n, ra, hr), BF16), vm((ra, width), F32),
            vm((rb, model), BF16), vm((slots, rb), BF16), vm((2, rb, slots), BF16),
            vm((slots // 2, lc), BF16), vm((ny, slots // 2, lc), BF16),
            vm((tp_n, slots, lc), BF16), vm((slots, hidden), BF16),
            vm((ny, slots, lc), BF16), vm((ny, slots, lc), BF16),
            vm((ny, slots, lc), BF16), vm((ny, slots, lc), BF16),
            vm((slots, lc), BF16), vm((slots, lc), BF16),
            vm((ny, rb, lc), BF16), vm((ny, rb, lc), BF16), vm((ny, rb, lc), BF16),
            vm((ny, rb, lc), BF16), vm((ny, rb, lc), BF16),
            dma((7,)), dma((n,)), dma((n,)), dma((n,)), dma((ny, n)), dma((ny, n)),
            dma((ny, n)), dma((ny, n)), dma((ny, n)), dma((ny, n)), dma((2,)), dma((ny,)), dma((ny,)),
            dma((ny,)), dma((ny,)), dma((ny, xs)), dma((ny, xs)), dma((ny,)), dma((ny,)),
            dma((ny,)), dma((ny,)), dma((ny,)), dma((ny,)),
            dma((2, ny)), dma((2, ny)), dma((ny, n)), dma((ny, n)), dma((n,)), dma((n,)),
        ],
        compiler_params=pltpu.CompilerParams(
            collective_id=0, has_side_effects=True, vmem_limit_bytes=64 * 1024 * 1000
        ),
        name="fused_layer",
    )(
        query_rows, key_rows, value_rows, q_gain, k_gain, table, mixer_gain.reshape(1, width),
        expert_input, expert_ids, gate_score, expert_gain.reshape(1, model),
        shared_gate, shared_up, shared_down, out_weight,
        gate_weight[0], up_weight[0], down_weight[0],
    )


def solution(mesh):
    in_specs = (
        P("ep", "tp"), P("ep", None), P("ep", None), P(), P(), P("tp", None), P(),
        P("ep", None), P("ep", None), P("ep", None), P(),
        P("ep", None, "tp"), P("ep", None, "tp"), P("ep", "tp", None),
        P(None, "tp"), P(None, "tp"), P("tp", None),
    )
    out_specs = (P("ep", None), P("ep", "tp"))
    return jax.shard_map(body, mesh=mesh, in_specs=in_specs, out_specs=out_specs, check_vma=False)
```

time: 122 us -> 89.6 us (0.73)
  Pallas kernels: 102 us -> 80.3 us
  other arithmetic: 9.51 us -> 1.39 us
  matrix products: 1.51 us -> 0 us
  local copies, waits for them, and re-layouts: 7.76 us -> 6.43 us
    pallas_call x1, Pallas kernels: 102 us -> 80.3 us  [body(): pl.pallas_call(functools.partial(fused_kernel, sizes), out_shape=(jax.Sha...]
    reduce_sum x5 -> x0, other arithmetic: 4.2 us -> none  [the longest x1 1.61 us: body(): jnp.mean(widened * widened, axis=1, keepdims=True) + EPSILON]
    pad x2 -> x0, local copies, waits for them, and re-layouts: 2.41 us -> none  [the longest x1 1.59 us: body(): jnp.pad(out_weight.reshape(heads, HEAD_DIM, width), ((0, 0), (HEAD_DIM, 0...]
    unnamed x24 -> x6, local copies, waits for them, and re-layouts: 4.29 us -> 6.43 us
    concatenate x3 -> x0, other arithmetic: 1.65 us -> none  [the longest x1 0.77 us: body(): kv_in = jnp.concatenate([key_rot.reshape(ra, HEAD_DIM), value_cols], axis=1)]
    dot_general x2 -> x0, matrix products: 1.51 us -> none  [the longest x1 1.28 us: body(): lax.dot_general(choose, own_cols, (((0,), (0,)), ((), ())), preferred_ele...]
    reshape x0 -> x1, other arithmetic: none -> 1.39 us  [body(): q_gain = jnp.concatenate([query_gain, query_gain]).reshape(1, 2 * HEAD_DIM)]
where the time goes in v2:
time: 89.6 us; the launch traced here: 88.8 us
  Pallas kernels  80.3 us (90%)
  local copies, waits for them, and re-layouts  6.43 us (7%)
  other arithmetic  1.39 us (2%)
    pallas_call x1, Pallas kernels, body(): pl.pallas_call(functools.partial(fused_kernel, sizes), out_shape=(jax.Sha...  80.3 us
    unnamed x6, local copies, waits for them, and re-layouts  6.43 us

profile of v2, /device:TPU:0, one launch (start us, length us, event | category | flops | bytes accessed | tf_op | source)
XLA Modules:
  0.0 88.8 jit_solution(4587460176477807195)
XLA Ops:
  0.6 1.4 %maximum_bitcast_fusion = (f32[1,128]{1,0:T(1,128)}, f32[1,128]{1,0:T(1,128)}) fusion(f32[64]{0:T(128)} %param.21, f32[64]{0:T(128)} %param.22), kind=kLoop, calls=%fused_computation | loop fusion | flops 256 | bytes 1536 | tf_op jit(solution)/shard_map/reshape | solution.py:574
  2.0 1.5 %copy.20.ids_ref = s32[256,2]{1,0:T(8,128)} copy(s32[256,2]{0,1:T(2,128)} %param.26) | data formatting | bytes 4096 | tf_op args[8]
  3.5 1.5 %copy.21.score_ref = f32[256,2]{1,0:T(8,128)} copy(f32[256,2]{0,1:T(2,128)} %param.27) | data formatting | bytes 4096 | tf_op args[9]
  5.0 80.3 %fused_layer.1 = (bf16[384,2048]{1,0:T(8,128)(2,1)}, bf16[256,512]{1,0:T(8,128)(2,1)}) custom-call(bf16[384,256]{1,0:T(8,128)(2,1)} %q_ref.1, bf16[384,256]{1,0:T(8,128)(2,1)} %k_ref.1, bf16[384,256]{1,0:T(8,128)(2,1)} %v_ref.1, f32[1,128]{1,0:T(1,128)} %get-tuple-element.2.qg_ref, f32[1,128]{1,0:T(1,128)} %get-tuple-element.3.kg_ref, ...), custom_call_target="tpu_custom_call" | custom-call | tf_op jit(solution)/shard_map/fused_layer/pallas_call | solution.py:586
  85.3 0.0 copy-start
  85.3 2.8 %copy.24 = bf16[384,2048]{1,0:T(8,128)(2,1)} copy(bf16[384,2048]{1,0:T(8,128)(2,1)} %get-tuple-element.6) | data formatting | bytes 3145728
  88.1 0.0 copy-done
  88.1 0.7 copy.25
Async XLA Ops:
  85.3 2.8 %copy-start = (bf16[256,512]{1,0:T(8,128)(2,1)S(1)}, bf16[256,512]{1,0:T(8,128)(2,1)}, u32[]{:S(2)}) copy-start(bf16[256,512]{1,0:T(8,128)(2,1)} %get-tuple-element.7) | copy-start | bytes 786436

commit v3 on v2

--- a/solution.py
+++ b/solution.py
@@ -33,6 +33,13 @@
         return [np.where(used, np.cos(angle), 0.0), np.where(used, np.sin(angle) * sign, 0.0)]
 
     return np.concatenate(pair(GRID_W, ~by_row) + pair(grid_rows, by_row)).astype(np.float32)
+
+
+def query_block(ra, total):
+    bq = max(16, min(ra, 128 * 3072 // total // 16 * 16))
+    while ra % bq:
+        bq -= 16
+    return bq
 
 
 def silu(v):
@@ -152,23 +159,23 @@
         tile = ow.at[rows(2 * by + side, hr)]
         return send(tile, tile, om_s.at[by], om_r.at[by], t=mate)
 
-    pl.semaphore_wait(barrier, n - 1 + ny - 1 + 1)
+    with jax.named_scope("barrier"):
+        pl.semaphore_wait(barrier, n - 1 + ny - 1 + 1)
 
     each(1, ny, lambda s: o_copy((y + s) % ny).start())
 
     x = x_ref[...].astype(F32)
     x_scale = lax.rsqrt(jnp.mean(x * x, axis=1, keepdims=True) + EPSILON)
     nrm[...] = (x * x_scale * xgain_ref[...]).astype(BF16)
-    elane = lax.broadcasted_iota(jnp.int32, (rb, 128), 1)
-    top = ids_ref.shape[1]
-    named = [ids_ref[:, k:k + 1] == elane for k in range(top)]
+    erow = lax.broadcasted_iota(jnp.int32, (128, rb), 0)
+    top = ids_ref.shape[0]
+    named = [ids_ref[k:k + 1, :] == erow for k in range(top)]
     member = named[0]
     for k in range(1, top):
         member = member | named[k]
-    earlier = lax.broadcasted_iota(jnp.int32, (rb, rb), 1) < lax.broadcasted_iota(jnp.int32, (rb, rb), 0)
-    rank = dot(jnp.where(earlier, 1.0, 0.0).astype(BF16), jnp.where(member, 1.0, 0.0).astype(BF16))
-    slot = jnp.where(member, rank, -1.0)
-    slot_t = slot.T
+    earlier = lax.broadcasted_iota(jnp.int32, (rb, rb), 0) < lax.broadcasted_iota(jnp.int32, (rb, rb), 1)
+    rank = dot(jnp.where(member, 1.0, 0.0).astype(BF16), jnp.where(earlier, 1.0, 0.0).astype(BF16))
+    slot_t = jnp.where(member, rank, -1.0)
     place = lax.broadcasted_iota(jnp.int32, (cp, rb), 0).astype(F32)
     for e in range(n):
         cht[e * cp:(e + 1) * cp, :] = jnp.where(slot_t[e:e + 1, :] == place, 1.0, 0.0).astype(BF16)
@@ -234,18 +241,19 @@
     k_own = jnp.where(odd, pltpu.roll(k_two, HEAD_DIM, 1), k_two)
     v_own = jnp.where(odd, v_two, pltpu.roll(v_two, HEAD_DIM, 1))
     k_sum = jnp.sum(jnp.where(left, k_own * k_own, 0.0), axis=1, keepdims=True)
-    k_turned = rotate(k_own * inverse_rms(k_sum) * kg_ref[...])
+    k_turned = rotate(k_own * inverse_rms(k_sum) * jnp.concatenate([kg_ref[...]] * 2, axis=1))
     kv_mine = jnp.where(left, k_turned, v_own).astype(BF16)
     kvo[...] = kv_mine
     kv[rows(me, ra), :] = kv_mine
 
     with jax.named_scope("queries"):
+        q_gain = jnp.concatenate([qg_ref[...]] * 2, axis=1)
         for p in range(pairs):
             q_two = q_ref[:, p * 128:(p + 1) * 128].astype(F32)
             square = q_two * q_two
             low = inverse_rms(jnp.sum(jnp.where(left, square, 0.0), axis=1, keepdims=True))
             high = inverse_rms(jnp.sum(jnp.where(left, 0.0, square), axis=1, keepdims=True))
-            turned = rotate(q_two * jnp.where(left, low, high) * qg_ref[...]) * HEAD_DIM ** (-0.5)
+            turned = rotate(q_two * jnp.where(left, low, high) * q_gain) * HEAD_DIM ** (-0.5)
             qs[2 * p * ra:(2 * p + 1) * ra, :] = jnp.where(left, turned, 0.0).astype(BF16)
             if 2 * p + 1 < heads:
                 qs[(2 * p + 1) * ra:(2 * p + 2) * ra, :] = jnp.where(
@@ -264,12 +272,14 @@
         each(1, xs, lambda t: kv_forward(src_z, t).start())
 
     with jax.named_scope("pick"):
-        total_score = score_ref[:, 0:1]
+        total_score = score_ref[0:1, :]
         for k in range(1, top):
-            total_score = total_score + score_ref[:, k:k + 1]
-        row_weight = jnp.zeros((rb, 128), F32)
+            total_score = total_score + score_ref[k:k + 1, :]
+        weight_t = jnp.zeros((128, rb), F32)
         for k in range(top):
-            row_weight = row_weight + jnp.where(named[k], score_ref[:, k:k + 1] / total_score * ROUTED_SCALE, 0.0)
+            weight_t = weight_t + jnp.where(named[k], score_ref[k:k + 1, :] / total_score * ROUTED_SCALE, 0.0)
+        row_weight = weight_t.T
+        slot = slot_t.T
         high_w = row_weight.astype(BF16)
         low_w = (row_weight - high_w.astype(F32)).astype(BF16)
         slot_lane = lax.broadcasted_iota(jnp.int32, (1, slots), 1).astype(F32)
@@ -313,7 +323,8 @@
 
     def far_pass(s):
         src = far_src(s)
-        d_far(src, me).wait_recv()
+        with jax.named_scope("fp"):
+            d_far(src, me).wait_recv()
         each(1, ny, lambda t: g_copy(y, (y + t) % ny, src).start())
         m_copy(y, src).start()
 
@@ -322,7 +333,8 @@
 
         def one(t):
             q = (y + t) % ny
-            g_copy(q, y, src).wait_recv()
+            with jax.named_scope("fpy"):
+                g_copy(q, y, src).wait_recv()
             m_copy(q, src).start()
 
         each(1, ny, one)
@@ -344,9 +356,7 @@
         each(1, ny, one)
 
     total = kv.shape[0]
-    bq = max(16, min(ra, 128 * 3072 // total // 16 * 16))
-    while ra % bq:
-        bq -= 16
+    bq = query_block(ra, total)
     per_head = ra // bq
 
     def attend(head, i):
@@ -357,28 +367,38 @@
         row_total = jnp.sum(exponent, axis=1, keepdims=True)
         return dot(exponent.astype(BF16), kv[...]) / row_total
 
-    turns = pairs * per_head
-
-    def attend_turn(i):
-        p = i // per_head
-        b = i % per_head
+    def attend_pair(p, b):
         first = attend(2 * p, b)
         if heads > 1:
             both = jnp.where(left, pltpu.roll(first, HEAD_DIM, 1), attend(2 * p + 1, b))
             attf[tp, rows(b, bq), rows(p, 128)] = both.astype(BF16)
         else:
             attf[tp, rows(b, bq), :] = first[:, HEAD_DIM:].astype(BF16)
-        each(i * hn // turns, (i + 1) * hn // turns, lambda s: finish_send(far_peer(s)))
-
-    def far_step(s):
-        far_pass(s)
-        each(jnp.maximum(s - 1, 0), s, far_pass_y)
-
-    def a_copy(by, q):
-        return send(attf.at[2 * by + core], attf.at[2 * by + core], a_s.at[q], a_r.at[by], t=2 * q + core)
-
-    def am_copy(by, side):
-        return send(attf.at[2 * by + side], attf.at[2 * by + side], am_s.at[by], am_r.at[by], t=mate)
+
+    def att_chunk(j, b):
+        return attf.at[j, rows(b, bq)]
+
+    def a_copy(by, q, b):
+        return send(
+            att_chunk(2 * by + core, b), att_chunk(2 * by + core, b), a_s.at[q, b], a_r.at[by, b], t=2 * q + core)
+
+    def am_copy(by, side, b):
+        return send(att_chunk(2 * by + side, b), att_chunk(2 * by + side, b), am_s.at[by, b], am_r.at[by, b], t=mate)
+
+    def att_pass(b):
+        def one(s):
+            by = (y + s) % ny
+            a_copy(by, y, b).wait_recv()
+            am_copy(by, core, b).start()
+
+        each(1, ny, one)
+
+    def attend_block(b):
+        each(0, pairs, lambda p: attend_pair(p, b))
+        each(1, ny, lambda s: a_copy(y, (y + s) % ny, b).start())
+        am_copy(y, core, b).start()
+        each(b * hn // per_head, (b + 1) * hn // per_head, lambda s: finish_send(far_peer(s)))
+        each(jnp.maximum(b - 1, 0), b, att_pass)
 
     ft = min(256, hid.shape[1])
 
@@ -434,28 +454,33 @@
 
     tiles = hid.shape[1] // ft
 
+    def arrive(s):
+        far_pass(s)
+        each(s, jnp.minimum(s + 1, hn - 1), lambda t: near_pass(t + 1))
+
     def near_tile(t):
         gate_up(near, t)
-        each(t * hn // tiles, (t + 1) * hn // tiles, far_step)
+        each(t * hn // tiles, (t + 1) * hn // tiles, far_pass_y)
 
     def far_tile(t):
         gate_up(far, t)
         each(1 + t * (zs - 1) // tiles, 1 + (t + 1) * (zs - 1) // tiles, kv_pass)
 
-    with jax.named_scope("near_pass"):
-        each(1, hn, near_pass)
+    with jax.named_scope("arrive"):
+        each(0, hn, arrive)
+    each(1, ny, lambda s: v_copy(y, (y + s) % ny).start())
+    each(1, zs, lambda s: kv_copy(me, z_peer(s)).start())
+    each(1, xs, lambda s: kv_copy(me, x_peer(s)).start())
     with jax.named_scope("near_wait"):
         weights[4].wait()
         weights[5].wait()
         each(1, hn, near_wait)
-    each(1, zs, lambda s: kv_copy(me, z_peer(s)).start())
-    each(1, xs, lambda s: kv_copy(me, x_peer(s)).start())
     with jax.named_scope("near_gate_up"):
         each(0, tiles, near_tile)
     with jax.named_scope("near_down"):
         weights[6].wait()
         each(1, ny + 1, lambda s: down_other(near, (y + s) % ny))
-        far_pass_y(hn - 1)
+    with jax.named_scope("near_down_own"):
         each(1, ny, lambda s: down_away(near, s))
         down_own(near, y)
     with jax.named_scope("far_wait"):
@@ -468,28 +493,20 @@
         each(1, ny + 1, lambda s: down_other(far, (y + s) % ny))
         each(1, ny, lambda s: down_away(far, s))
         down_own(far, y)
-    each(1, ny, lambda s: v_copy(y, (y + s) % ny).start())
+    with jax.named_scope("kv_rest"):
+        each(1, xs, kv_rest)
+    with jax.named_scope("attend"):
+        each(0, per_head, attend_block)
     with jax.named_scope("finish_near"):
         each(1, hn, lambda s: finish_send(near_peer(s)))
         ret[rows(me, cp), :] = finish(me)
-    with jax.named_scope("kv_rest"):
-        each(1, xs, kv_rest)
-    with jax.named_scope("attend"):
-        each(0, turns, attend_turn)
-    am_copy(y, core).start()
-    each(1, ny, lambda s: a_copy(y, (y + s) % ny).start())
-
+    with jax.named_scope("att_wait"):
+        att_pass(per_head - 1)
     with jax.named_scope("ow_last"):
         ow_last()
-    with jax.named_scope("att_wait"):
-        def att_pass(s):
-            by = (y + s) % ny
-            a_copy(by, y).wait_recv()
-            am_copy(by, core).start()
-
-        each(1, ny, att_pass)
+
     with jax.named_scope("mixer"):
-        each(0, ny, lambda by: am_copy(by, other).wait_recv())
+        each(0, ny, lambda by: each(0, per_head, lambda b: am_copy(by, other, b).wait_recv()))
         each(0, ny, lambda by: om_copy(by, other).wait_recv())
         width = mix.shape[1]
         tile = min(512, width)
@@ -529,7 +546,7 @@
         q = (y + s) % ny
         o_copy(q).wait_send()
         each(1, xs, lambda t: ox_copy(q, (my_x + t) % xs).wait_send())
-        a_copy(y, q).wait_send()
+        each(0, per_head, lambda b: a_copy(y, q, b).wait_send())
         v_copy(y, q).wait_send()
         u_copy(y, q, me).wait_send()
 
@@ -543,8 +560,17 @@
         sh_copy.wait_send()
         each(0, ny, lambda q: each(0, 2, lambda hf: p_copy(hf, q).wait_send()))
         each(0, ny, lambda by: om_copy(by, core).wait_send())
-        each(0, ny, lambda by: am_copy(by, core).wait_send())
+        each(0, ny, lambda by: each(0, per_head, lambda b: am_copy(by, core, b).wait_send()))
         each(1, ny, drain_y)
+
+
+def store_kernel(mixed_ref, expert_ref, mixed_out, expert_out, sems):
+    first = pltpu.make_async_copy(mixed_ref, mixed_out, sems.at[0])
+    second = pltpu.make_async_copy(expert_ref, expert_out, sems.at[1])
+    first.start()
+    second.start()
+    first.wait()
+    second.wait()
 
 
 def body(
@@ -571,24 +597,20 @@
         query_rows = jnp.pad(query_rows, ((0, 0), (0, HEAD_DIM)))
     pairs = -(-heads // 2)
     table = jnp.asarray(position_tables(n * ra // GRID_W))
-    q_gain = jnp.concatenate([query_gain, query_gain]).reshape(1, 2 * HEAD_DIM)
-    k_gain = jnp.concatenate([key_gain, key_gain]).reshape(1, 2 * HEAD_DIM)
 
     slots = n * cp
     hidden = gate_weight.shape[2]
     sh = shared_gate.shape[1]
     hr = heads * HEAD_DIM
+    blocks = ra // query_block(ra, n * ra)
     vm = pltpu.VMEM
     dma = pltpu.SemaphoreType.DMA
     vspec = pl.BlockSpec(memory_space=pltpu.VMEM)
     hspec = pl.BlockSpec(memory_space=pl.ANY)
     sizes = (n, tp_n, ny, heads, cp, lc, xs)
-    return pl.pallas_call(
+    mixed, expert = pl.pallas_call(
         functools.partial(fused_kernel, sizes),
-        out_shape=(
-            jax.ShapeDtypeStruct((ra, width), BF16),
-            jax.ShapeDtypeStruct((rb, lc), BF16),
-        ),
+        out_shape=(pltpu.VMEM((ra, width), BF16), pltpu.VMEM((rb, lc), BF16)),
         in_specs=[vspec] * 11 + [hspec] * 7,
         out_specs=(vspec, vspec),
         scratch_shapes=[
@@ -609,19 +631,30 @@
             dma((7,)), dma((n,)), dma((n,)), dma((n,)), dma((ny, n)), dma((ny, n)),
             dma((ny, n)), dma((ny, n)), dma((ny, n)), dma((ny, n)), dma((2,)), dma((ny,)), dma((ny,)),
             dma((ny,)), dma((ny,)), dma((ny, xs)), dma((ny, xs)), dma((ny,)), dma((ny,)),
-            dma((ny,)), dma((ny,)), dma((ny,)), dma((ny,)),
+            dma((ny, blocks)), dma((ny, blocks)), dma((ny, blocks)), dma((ny, blocks)),
             dma((2, ny)), dma((2, ny)), dma((ny, n)), dma((ny, n)), dma((n,)), dma((n,)),
         ],
         compiler_params=pltpu.CompilerParams(
-            collective_id=0, has_side_effects=True, vmem_limit_bytes=64 * 1024 * 1000
+            collective_id=0, has_side_effects=True, vmem_limit_bytes=56 * 1024 * 1024
         ),
         name="fused_layer",
     )(
-        query_rows, key_rows, value_rows, q_gain, k_gain, table, mixer_gain.reshape(1, width),
-        expert_input, expert_ids, gate_score, expert_gain.reshape(1, model),
+        query_rows, key_rows, value_rows, query_gain.reshape(1, HEAD_DIM), key_gain.reshape(1, HEAD_DIM), table, mixer_gain.reshape(1, width),
+        expert_input, expert_ids.T, gate_score.T, expert_gain.reshape(1, model),
         shared_gate, shared_up, shared_down, out_weight,
         gate_weight[0], up_weight[0], down_weight[0],
     )
+    return pl.pallas_call(
+        store_kernel,
+        out_shape=(
+            jax.ShapeDtypeStruct((ra, width), BF16),
+            jax.ShapeDtypeStruct((rb, lc), BF16),
+        ),
+        in_specs=[vspec, vspec],
+        out_specs=(hspec, hspec),
+        scratch_shapes=[dma((2,))],
+        name="store",
+    )(pltpu.with_memory_space_constraint(mixed, pltpu.VMEM), pltpu.with_memory_space_constraint(expert, pltpu.VMEM))
 
 
 def solution(mesh):

time: 89.6 us -> 75.3 us (0.84)
  local copies, waits for them, and re-layouts: 6.43 us -> 0 us
  Pallas kernels: 80.3 us -> 74.5 us
  other arithmetic: 1.39 us -> 0 us
    unnamed x6 -> x0, local copies, waits for them, and re-layouts: 6.43 us -> none
    pallas_call x1 -> x2, Pallas kernels: 80.3 us -> 74.5 us  [the longest x1 73.3 us: body(): pl.pallas_call(functools.partial(fused_kernel, sizes), out_shape=(pltpu.V...]
    reshape x1 -> x0, other arithmetic: 1.39 us -> none  [body(): q_gain = jnp.concatenate([query_gain, query_gain]).reshape(1, 2 * HEAD_DIM)]
where the time goes in v3:
time: 75.3 us; the launch traced here: 75.2 us
  Pallas kernels  74.5 us (99%)
    pallas_call x1, Pallas kernels, body(): pl.pallas_call(functools.partial(fused_kernel, sizes), out_shape=(pltpu.V...  73.3 us

profile of v3, /device:TPU:0, one launch (start us, length us, event | category | flops | bytes accessed | tf_op | source)
XLA Modules:
  0.0 75.2 jit_solution(12716045333371015847)
XLA Ops:
  0.6 73.3 %fused_layer.1 = (bf16[384,2048]{1,0:T(8,128)(2,1)S(1)}, bf16[256,512]{1,0:T(8,128)(2,1)S(1)}) custom-call(bf16[384,256]{1,0:T(8,128)(2,1)} %q_ref.1, bf16[384,256]{1,0:T(8,128)(2,1)} %k_ref.1, bf16[384,256]{1,0:T(8,128)(2,1)} %v_ref.1, f32[1,64]{1,0:T(1,128)} %bitcast.16, f32[1,64]{1,0:T(1,128)} %bitcast.17, f32[224,128]{1,0:T(8,128)} %constant.2.clone.table_ref, ...), custom_call_target="tpu_custom_call" | custom-call | tf_op jit(solution)/shard_map/fused_layer/pallas_call | solution.py:611
  73.9 1.2 %store.1 = (bf16[384,2048]{1,0:T(8,128)(2,1)}, bf16[256,512]{1,0:T(8,128)(2,1)}) custom-call(bf16[384,2048]{1,0:T(8,128)(2,1)S(1)} %get-tuple-element.4.mixed_ref, bf16[256,512]{1,0:T(8,128)(2,1)S(1)} %get-tuple-element.5.expert_ref), custom_call_target="tpu_custom_call" | custom-call | tf_op jit(solution)/shard_map/store/pallas_call | solution.py:647

commit v4 on v3

--- a/solution.py
+++ b/solution.py
@@ -36,7 +36,7 @@
 
 
 def query_block(ra, total):
-    bq = max(16, min(ra, 128 * 3072 // total // 16 * 16))
+    bq = max(16, min(ra, 192 * 3072 // total // 16 * 16))
     while ra % bq:
         bq -= 16
     return bq
@@ -464,11 +464,9 @@
 
     def far_tile(t):
         gate_up(far, t)
-        each(1 + t * (zs - 1) // tiles, 1 + (t + 1) * (zs - 1) // tiles, kv_pass)
 
     with jax.named_scope("arrive"):
         each(0, hn, arrive)
-    each(1, ny, lambda s: v_copy(y, (y + s) % ny).start())
     each(1, zs, lambda s: kv_copy(me, z_peer(s)).start())
     each(1, xs, lambda s: kv_copy(me, x_peer(s)).start())
     with jax.named_scope("near_wait"):
@@ -483,20 +481,23 @@
     with jax.named_scope("near_down_own"):
         each(1, ny, lambda s: down_away(near, s))
         down_own(near, y)
+    with jax.named_scope("kv_pass"):
+        each(1, zs, kv_pass)
     with jax.named_scope("far_wait"):
         each(0, hn, far_wait)
     with jax.named_scope("far_gate_up"):
         each(0, tiles, far_tile)
-    with jax.named_scope("ow_pass"):
-        ow_pass()
     with jax.named_scope("far_down"):
         each(1, ny + 1, lambda s: down_other(far, (y + s) % ny))
         each(1, ny, lambda s: down_away(far, s))
         down_own(far, y)
     with jax.named_scope("kv_rest"):
         each(1, xs, kv_rest)
+    with jax.named_scope("ow_pass"):
+        ow_pass()
     with jax.named_scope("attend"):
         each(0, per_head, attend_block)
+    each(1, ny, lambda s: v_copy(y, (y + s) % ny).start())
     with jax.named_scope("finish_near"):
         each(1, hn, lambda s: finish_send(near_peer(s)))
         ret[rows(me, cp), :] = finish(me)

time: 75.3 us -> 71.3 us (0.947)
  Pallas kernels: 74.5 us -> 70.5 us
    pallas_call x1, Pallas kernels: 73.3 us -> 69.3 us  [body(): pl.pallas_call(functools.partial(fused_kernel, sizes), out_shape=(pltpu.V...]
where the time goes in v4:
time: 71.3 us; the launch traced here: 71.2 us
  Pallas kernels  70.5 us (99%)
    pallas_call x1, Pallas kernels, body(): pl.pallas_call(functools.partial(fused_kernel, sizes), out_shape=(pltpu.V...  69.3 us

profile of v4, /device:TPU:0, one launch (start us, length us, event | category | flops | bytes accessed | tf_op | source)
XLA Modules:
  0.0 71.2 jit_solution(15628825387764023172)
XLA Ops:
  0.6 69.3 %fused_layer.1 = (bf16[384,2048]{1,0:T(8,128)(2,1)S(1)}, bf16[256,512]{1,0:T(8,128)(2,1)S(1)}) custom-call(bf16[384,256]{1,0:T(8,128)(2,1)} %q_ref.1, bf16[384,256]{1,0:T(8,128)(2,1)} %k_ref.1, bf16[384,256]{1,0:T(8,128)(2,1)} %v_ref.1, f32[1,64]{1,0:T(1,128)} %bitcast.16, f32[1,64]{1,0:T(1,128)} %bitcast.17, f32[224,128]{1,0:T(8,128)} %constant.2.clone.table_ref, ...), custom_call_target="tpu_custom_call" | custom-call | tf_op jit(solution)/shard_map/fused_layer/pallas_call | solution.py:612
  69.9 1.2 %store.1 = (bf16[384,2048]{1,0:T(8,128)(2,1)}, bf16[256,512]{1,0:T(8,128)(2,1)}) custom-call(bf16[384,2048]{1,0:T(8,128)(2,1)S(1)} %get-tuple-element.4.mixed_ref, bf16[256,512]{1,0:T(8,128)(2,1)S(1)} %get-tuple-element.5.expert_ref), custom_call_target="tpu_custom_call" | custom-call | tf_op jit(solution)/shard_map/store/pallas_call | solution.py:648
